TPU v7x, 512 devices: a whole 4x8x8 slice. The times are simulated.
512 devices in a mesh: dp: 4 (over x), kv: 64 (over z, y), tp: 2 (over core).
Axes of the slice: x: 4, y: 8, z: 8, core: 2. Of those that a mesh axis runs over, the one named last changes fastest.
Arguments:
- tokens: bfloat16 [16, 4096], P('dp', ('kv', 'tp')), may hold values from -11 to 11
- attn_gain: float32 [4096], replicated, may hold values from 0.1 to 1.9
- query_weight: bfloat16 [4096, 4096], P('kv', 'tp'), may hold values from -0.09375 to 0.09375
- key_cache: bfloat16 [16, 16384, 2, 128], P('dp', 'kv', 'tp'), may hold values from -820 to 820
- value_cache: bfloat16 [16, 16384, 2, 128], P('dp', 'kv', 'tp'), may hold values from -6 to 6
- head_lambda: float32 [32], P('tp'), may hold values from 0.3 to 0.8
- head_gain: float32 [128], replicated, may hold values from 0.1 to 1.9
- out_weight: bfloat16 [4096, 4096], P('kv', 'tp'), may hold values from -0.09375 to 0.09375
- mlp_gain: float32 [4096], replicated, may hold values from 0.1 to 1.9
- gate_weight: bfloat16 [11264, 4096], P(('kv', 'tp')), may hold values from -0.09375 to 0.09375
- up_weight: bfloat16 [11264, 4096], P(('kv', 'tp')), may hold values from -0.09375 to 0.09375
- down_weight: bfloat16 [11264, 4096], P(('kv', 'tp')), may hold values from -0.21875 to 0.21875
Outputs:
- mixed: bfloat16 [16, 4096], P('dp', ('kv', 'tp'))
All inputs are finite; a program needn't handle non-finite values.
Results may differ from a plain program's by a relative error of at most 0.02.
The roundings to bfloat16 on the way count: a program that leaves them out, or rounds other values in their place, can miss the bound.
Values may be sent and summed in bfloat16 or wider, within the bound.
No kernel may reach another device: no remote copies, remote signals or barrier semaphores. Data moves between devices by JAX's collectives and lax.ppermute only.
A program may use at most 64 MiB of HBM per device.

v0:
```python
import jax
import jax.numpy as jnp
from jax import lax
from jax.sharding import Mesh
from jax.sharding import PartitionSpec as P

KV = ("kv_0", "kv_1")
KV_TP = ("kv_0", "kv_1", "tp")


EPS = 1e-06
THETA = 10000.0


def sent_to_all(x, axis):
    copies = jnp.broadcast_to(x, (lax.axis_size(axis), *x.shape))
    return lax.all_to_all(copies, axis, split_axis=0, concat_axis=0, tiled=True)


def joined_along(pieces, dim):
    shape = list(pieces.shape[1:])
    shape[dim] *= pieces.shape[0]
    return jnp.moveaxis(pieces, 0, dim).reshape(shape)


def whole_of(x, axes, dim):
    far, near = axes
    first = sent_to_all(x, far)
    pieces = jnp.swapaxes(sent_to_all(first, near), 0, 1)
    return joined_along(pieces.reshape(-1, *x.shape), dim)


def one_axis_at_a_time(x, axes):
    for axis in axes:
        x = lax.psum(x, axis)
    return x


def collected_together(x, axis):
    leaves = jax.tree.leaves(x)
    turns = sorted(range(len(leaves)), key=lambda k: -leaves[k].size)
    width = (1, *leaves[turns[0]].shape)[-1]
    lines = [
        jnp.pad(leaves[k].reshape(-1), (0, -leaves[k].size % width)).reshape(-1, width)
        for k in turns
    ]
    both, at, found = (lax.all_gather(jnp.concatenate(lines), axis), 0, {})
    for k, line in zip(turns, lines):
        slab = both[:, at : at + len(line)].reshape(len(both), -1)
        found[k] = slab[:, : leaves[k].size].reshape(-1, *leaves[k].shape)
        at += len(line)
    numbers = iter(range(len(leaves)))
    return jax.tree.map(lambda _: found[next(numbers)], x)


def merged_by_axis(x, axes, combine):
    for axis in axes:
        pieces = collected_together(x, axis)
        x = jax.tree.map(lambda part: part[0], pieces)
        for k in range(1, lax.axis_size(axis)):
            x = combine(x, jax.tree.map(lambda part: part[k], pieces))
    return x


def split_up(x, dim, count):
    shape = x.shape
    pieces = x.reshape(*shape[:dim], count, shape[dim] // count, *shape[dim + 1 :])
    return jnp.moveaxis(pieces, dim, 0)


def sum_at_owner(x, axis, dim):
    count = lax.axis_size(axis)
    pieces = lax.all_to_all(split_up(x, dim, count), axis, 0, 0, tiled=True)
    return jnp.sum(pieces, axis=0)


def sum_by_axis(x, axes, dim):
    far, near = axes
    own = sum_at_owner(split_up(x, dim, lax.axis_size(far)), near, dim + 1)
    return jnp.sum(lax.all_to_all(own, far, 0, 0, tiled=True), axis=0)


def rotate(vector, position):
    half_len = vector.shape[-1] // 2
    inv_freq = 1.0 / THETA ** (jnp.arange(half_len, dtype=jnp.float32) / half_len)
    angles = position * inv_freq
    cos_table = jnp.cos(angles)
    sin_table = jnp.sin(angles)
    first_half = vector[..., :half_len]
    second_half = vector[..., half_len:]
    return jnp.concatenate(
        [
            first_half * cos_table - second_half * sin_table,
            second_half * cos_table + first_half * sin_table,
        ],
        axis=-1,
    )


def combine(earlier, latter):
    peak_a, total_a, value_a = earlier
    peak_b, total_b, value_b = latter
    peak_new = jnp.maximum(peak_a, peak_b)
    factor_a = jnp.exp(peak_a - peak_new)
    factor_b = jnp.exp(peak_b - peak_new)
    return (
        peak_new,
        total_a * factor_a + total_b * factor_b,
        value_a * factor_a[..., None] + value_b * factor_b[..., None],
    )


def inner_last(left, right):
    return lax.dot_general(
        left, right, (((1,), (1,)), ((), ())), preferred_element_type=jnp.float32
    )


def shards(
    tokens,
    attn_gain,
    query_weight,
    key_cache,
    value_cache,
    head_lambda,
    head_gain,
    out_weight,
    mlp_gain,
    gate_weight,
    up_weight,
    down_weight,
):
    row_count = tokens.shape[0]
    kv_count = lax.axis_size(KV)
    tp_count = lax.axis_size("tp")
    kv_index = lax.axis_index(KV)
    row_span = query_weight.shape[0]
    full_rows = whole_of(tokens, (("kv_0", "kv_1"), "tp"), 1)
    wide_rows = full_rows.astype(jnp.float32)
    mean_square = jnp.mean(wide_rows * wide_rows, axis=-1, keepdims=True)
    scaled = (wide_rows * attn_gain).astype(jnp.bfloat16)
    local_cols = lax.dynamic_slice_in_dim(scaled, kv_index * row_span, row_span, 1)
    queries = one_axis_at_a_time(
        jnp.dot(local_cols, query_weight, preferred_element_type=jnp.float32), KV
    )
    queries = queries * lax.rsqrt(mean_square + EPS)
    head_count = head_lambda.shape[0]
    kv_local = key_cache.shape[2]
    group_size = head_count // kv_local
    position_count = key_cache.shape[1]
    half_dim = key_cache.shape[3] // 2
    value_dim = value_cache.shape[3]
    queries = queries.reshape(row_count, kv_local, group_size, 2, half_dim)
    rotated = rotate(queries, jnp.float32(position_count * kv_count)).astype(jnp.bfloat16)
    key_grid = key_cache.reshape(row_count, position_count, kv_local, 2, half_dim)
    scores = jnp.einsum(
        "bkgch,bpkch->bkgcp", rotated, key_grid, preferred_element_type=jnp.float32
    ) * half_dim ** (-0.5)
    local_peak = jnp.max(scores, axis=-1)
    weights_exp = jnp.exp(scores - local_peak[..., None])
    lam_grid = head_lambda.reshape(kv_local, group_size)[None, :, :, None]
    exp_total = jnp.sum(weights_exp, axis=-1)
    weighted = jnp.einsum(
        "bkgcp,bpkv->bkgcv",
        weights_exp.astype(jnp.bfloat16),
        value_cache,
        preferred_element_type=jnp.float32,
    )
    peak_all, total_all, weighted_all = merged_by_axis(
        (local_peak, exp_total, weighted), KV, combine
    )
    attended = weighted_all / total_all[..., None]
    difference = attended[:, :, :, 0] - lam_grid * attended[:, :, :, 1]
    head_norm = lax.rsqrt(jnp.mean(difference * difference, axis=-1, keepdims=True) + EPS)
    head_out = (difference * head_norm * head_gain).reshape(row_count, head_count * value_dim)
    head_out = head_out.astype(jnp.bfloat16)
    out_part = inner_last(head_out, out_weight).astype(jnp.bfloat16)
    pieces = whole_of(out_part, (("kv_0", "kv_1"), "tp"), 1)
    attention = jnp.sum(
        pieces.astype(jnp.float32).reshape(row_count, kv_count, tp_count, -1), axis=2
    )
    stream = wide_rows + attention.reshape(row_count, -1)
    stream_square = jnp.mean(stream * stream, axis=-1, keepdims=True)
    normed = (stream * lax.rsqrt(stream_square + EPS) * mlp_gain).astype(jnp.bfloat16)
    gate_out = inner_last(normed, gate_weight)
    up_out = inner_last(normed, up_weight)
    hidden = (jax.nn.silu(gate_out) * up_out).astype(jnp.bfloat16)
    own_cols = tokens.shape[1]
    down_cols = sum_by_axis(
        lax.dot_general(
            down_weight, hidden, (((0,), (1,)), ((), ())), preferred_element_type=jnp.float32
        ),
        (("kv_0", "kv_1"), "tp"),
        0,
    )
    column_index = lax.axis_index(KV_TP)
    own_stream = lax.dynamic_slice_in_dim(stream, column_index * own_cols, own_cols, 1)
    return (own_stream + down_cols.T).astype(jnp.bfloat16)


def solution(mesh):
    torus = Mesh(
        mesh.devices.reshape(mesh.shape["dp"], 8, 8, mesh.shape["tp"]), ("dp", "kv_0", "kv_1", "tp")
    )
    in_specs = (
        P("dp", KV_TP),
        P(),
        P(KV, "tp"),
        P("dp", KV, "tp", None),
        P("dp", KV, "tp", None),
        P("tp"),
        P(),
        P(KV, "tp"),
        P(),
        P(KV_TP, None),
        P(KV_TP, None),
        P(KV_TP, None),
    )
    out_specs = P("dp", KV_TP)
    return jax.shard_map(
        shards, mesh=torus, in_specs=in_specs, out_specs=out_specs, check_vma=False
    )
```

profile of v0, /device:TPU:1, one launch (start us, length us, event | category | flops | bytes accessed | tf_op | source)
XLA Modules:
  0.0 199.4 jit_solution(2808983307863396402)
XLA Ops:
  0.0 1.4 broadcast_in_dim.8
  1.4 17.3 %all-to-all-start = ((bf16[64,4,32]{2,1,0:T(4,128)(2,1)}), bf16[64,4,32]{2,1,0:T(4,128)(2,1)S(1)}, u32[]{:S(2)}, u32[]{:S(2)}) async-start(bf16[64,4,32]{2,1,0:T(4,128)(2,1)} %broadcast_in_dim.8), calls=%async_computation | async-start | bytes 131072 | tf_op jit(solution)/shard_map/all_to_all | solution.py:17
  18.8 1.1 copy.28
  19.9 0.8 dynamic-slice
  20.7 9.1 %all-to-all-done = bf16[64,4,32]{2,1,0:T(4,128)(2,1)S(1)} async-done(((bf16[64,4,32]{2,1,0:T(4,128)(2,1)}), bf16[64,4,32]{2,1,0:T(4,128)(2,1)S(1)}, u32[]{:S(2)}, u32[]{:S(2)}) %all-to-all-start) | async-done | bytes 16416 | tf_op jit(solution)/shard_map/all_to_all | solution.py:17
  30.0 5.5 %all_to_all.30 = bf16[2,2,4096]{2,1,0:T(2,128)(2,1)S(1)} all-to-all(bf16[2,2,4096]{2,1,0:T(2,128)(2,1)S(1)} %reshape.2089), channel_id=1, replica_groups=mesh['dp'=4,'kv_0'=8,'kv_1'=8,'tp'=2] {'tp'}, dimensions={0} | all-to-all | bytes 65536 | tf_op jit(solution)/shard_map/all_to_all | solution.py:17
  36.1 0.7 copy-done.4
  36.7 0.2 fusion.48
  36.9 20.3 %psum.14 = f32[4,2048]{1,0:T(4,128)S(1)} all-reduce(f32[4,2048]{1,0:T(4,128)S(1)} %fusion.48), channel_id=1, replica_groups=mesh['dp'=4,'kv_0'=8,'kv_1'=8,'tp'=2] {'kv_0'}, use_global_device_ids=true, to_apply=%region_0.0 | all-reduce | flops 8192 | bytes 65536 | tf_op jit(solution)/shard_map/psum | solution.py:35
  57.2 20.5 %psum.15 = f32[4,2048]{1,0:T(4,128)S(1)} all-reduce(f32[4,2048]{1,0:T(4,128)S(1)} %psum.14), channel_id=1, replica_groups=mesh['dp'=4,'kv_0'=8,'kv_1'=8,'tp'=2] {'kv_1'}, use_global_device_ids=true, to_apply=%region_1.0 | all-reduce | flops 8192 | bytes 65536 | tf_op jit(solution)/shard_map/psum | solution.py:35
  78.1 0.3 fusion.100
  79.1 0.2 fusion.2
  79.4 18.9 %all-gather.2 = f32[8,130,128]{2,1,0:T(8,128)S(1)} all-gather(f32[1,130,128]{2,1,0:T(8,128)S(1)} %maximum_bitcast_fusion), channel_id=2, replica_groups=mesh['dp'=4,'kv_0'=8,'kv_1'=8,'tp'=2] {'kv_0'}, dimensions={0}, use_global_device_ids=true | all-gather | bytes 599040 | tf_op jit(solution)/shard_map/all_gather | solution.py:47
  98.5 0.3 fusion.9
  98.8 19.4 %all-gather.3 = f32[8,130,128]{2,1,0:T(8,128)S(1)} all-gather(f32[1,130,128]{2,1,0:T(8,128)S(1)} %maximum_bitcast_fusion.1), channel_id=3, replica_groups=mesh['dp'=4,'kv_0'=8,'kv_1'=8,'tp'=2] {'kv_1'}, dimensions={0}, use_global_device_ids=true | all-gather | bytes 599040 | tf_op jit(solution)/shard_map/all_gather | solution.py:47
  120.7 1.2 add_divide_fusion
  122.3 0.6 copy-done.5
  123.2 17.5 %all_to_all.31 = bf16[64,2,128]{2,1,0:T(2,128)(2,1)S(1)} all-to-all(bf16[64,2,128]{2,1,0:T(2,128)(2,1)S(1)} %reshape.2091), channel_id=1, replica_groups=mesh['dp'=4,'kv_0'=8,'kv_1'=8,'tp'=2] {'kv_0','kv_1'}, dimensions={0} | all-to-all | bytes 65536 | tf_op jit(solution)/shard_map/all_to_all | solution.py:17
  141.0 31.9 %all_to_all.32 = bf16[2,2,8192]{2,1,0:T(2,128)(2,1)S(1)} all-to-all(bf16[2,2,8192]{2,1,0:T(2,128)(2,1)S(1)} %reshape.2093), channel_id=1, replica_groups=mesh['dp'=4,'kv_0'=8,'kv_1'=8,'tp'=2] {'tp'}, dimensions={0} | all-to-all | bytes 131072 | tf_op jit(solution)/shard_map/all_to_all | solution.py:17
  173.1 0.4 bitcast_reduce_fusion
  173.9 0.7 copy-done.1
  174.6 0.3 fusion.95
  174.9 0.7 convolution_bitcast_fusion
  175.7 0.3 reshape_reshape.2
  176.2 3.8 %all_to_all.33 = f32[2,1,8192]{2,1,0:T(1,128)S(1)} all-to-all(f32[2,1,8192]{2,1,0:T(1,128)S(1)} %reshape.2095), channel_id=1, replica_groups=mesh['dp'=4,'kv_0'=8,'kv_1'=8,'tp'=2] {'tp'}, dimensions={0} | all-to-all | bytes 131072 | tf_op jit(solution)/shard_map/all_to_all | solution.py:73
  180.0 0.5 broadcast.362
  180.5 0.8 reduce.224
  181.6 0.7 reshape.2097
  182.4 4.6 %all-to-all-start.5 = ((f32[64,1,128]{2,1,0:T(1,128)}), f32[64,1,128]{2,1,0:T(1,128)S(1)}, u32[]{:S(2)}, u32[]{:S(2)}) async-start(f32[64,1,128]{2,1,0:T(1,128)} %reshape.2097), calls=%async_computation.5 | async-start | bytes 65536 | tf_op jit(solution)/shard_map/all_to_all | solution.py:80
  187.0 10.8 %all-to-all-done.5 = f32[64,1,128]{2,1,0:T(1,128)S(1)} async-done(((f32[64,1,128]{2,1,0:T(1,128)}), f32[64,1,128]{2,1,0:T(1,128)S(1)}, u32[]{:S(2)}, u32[]{:S(2)}) %all-to-all-start.5) | async-done | bytes 32800 | tf_op jit(solution)/shard_map/all_to_all | solution.py:80
  197.8 0.7 reduce.225
  198.8 0.6 fusion.44
  (88 shorter events, 6.6 us)
Async XLA Ops:
  0.0 174.9 %copy-start = (bf16[88,4096]{1,0:T(8,128)(2,1)S(1)}, bf16[88,4096]{1,0:T(8,128)(2,1)}, u32[]{:S(2)}) copy-start(bf16[88,4096]{1,0:T(8,128)(2,1)} %param.23) | copy-start | bytes 2162692
  1.4 17.3 %copy-start.7 = (f32[16]{0:T(128)S(1)}, f32[16]{0:T(128)}, u32[]{:S(2)}) copy-start(f32[16]{0:T(128)} %param.17) | copy-start | bytes 196
  1.4 17.3 %copy-start.8 = (f32[128]{0:T(128)S(1)}, f32[128]{0:T(128)}, u32[]{:S(2)}) copy-start(f32[128]{0:T(128)} %param.18) | copy-start | bytes 1540
  1.4 28.3 %all-to-all-start = ((bf16[64,4,32]{2,1,0:T(4,128)(2,1)}), bf16[64,4,32]{2,1,0:T(4,128)(2,1)S(1)}, u32[]{:S(2)}, u32[]{:S(2)}) async-start(bf16[64,4,32]{2,1,0:T(4,128)(2,1)} %broadcast_in_dim.8), calls=%async_computation | async-start | bytes 131072 | tf_op jit(solution)/shard_map/all_to_all | solution.py:17
  35.8 1.0 copy-start.4
  78.1 1.0 copy-start.3
  121.9 1.0 copy-start.5
  173.5 1.1 copy-start.1
  173.6 1.0 copy-start.6
  173.7 1.2 copy-start.2
  182.4 15.5 %all-to-all-start.5 = ((f32[64,1,128]{2,1,0:T(1,128)}), f32[64,1,128]{2,1,0:T(1,128)S(1)}, u32[]{:S(2)}, u32[]{:S(2)}) async-start(f32[64,1,128]{2,1,0:T(1,128)} %reshape.2097), calls=%async_computation.5 | async-start | bytes 65536 | tf_op jit(solution)/shard_map/all_to_all | solution.py:80
where the time goes:
time: 200 us; the launch traced here: 199 us
  blocking collectives  138 us (69%)
  starting transfers between devices  21.9 us (11%)
  waiting for transfers between devices  19.9 us (10%)
  local copies, waits for them, and re-layouts  12 us (6%)
  other arithmetic  5.28 us (3%)
    all_to_all x3, blocking collectives, sent_to_all(): return lax.all_to_all(copies, axis, split_axis=0, concat_axis=0, tiled=True)  54.9 us
    psum x2, blocking collectives, one_axis_at_a_time(): x = lax.psum(x, axis)  40.8 us
    all_gather x2, blocking collectives, collected_together(): both, at, found = (lax.all_gather(jnp.concatenate(lines), axis), 0, {})  38.3 us
    all_to_all x1, starting transfers between devices, sent_to_all(): return lax.all_to_all(copies, axis, split_axis=0, concat_axis=0, tiled=True)  17.3 us
    all_to_all x1, waiting for transfers between devices, sum_by_axis(): return jnp.sum(lax.all_to_all(own, far, 0, 0, tiled=True), axis=0)  10.8 us
    all_to_all x1, waiting for transfers between devices, sent_to_all(): return lax.all_to_all(copies, axis, split_axis=0, concat_axis=0, tiled=True)  9.06 us
    unnamed x32, local copies, waits for them, and re-layouts  5 us
    all_to_all x1, starting transfers between devices, sum_by_axis(): return jnp.sum(lax.all_to_all(own, far, 0, 0, tiled=True), axis=0)  4.61 us
  transfers between devices with their start and end apart: 2, of which 2 were waited for; matrix products, arithmetic and copies ran while one was open for 1% of the time, Pallas kernels for 0%

commit v1 on v0

v1 whole, which is shorter than its diff:
```python
import jax
import jax.numpy as jnp
from jax import lax
from jax.experimental import pallas as pl
from jax.experimental.pallas import tpu as pltpu
from jax.sharding import Mesh
from jax.sharding import PartitionSpec as P

KV = ("kv_0", "kv_1")
KV_TP = ("kv_0", "kv_1", "tp")
EPS = 1e-06
THETA = 10000.0
F32 = jnp.float32
BF16 = jnp.bfloat16
SHAPE = jax.ShapeDtypeStruct


def lanes(shape):
    return lax.broadcasted_iota(jnp.int32, shape, len(shape) - 1)


def rows(shape):
    return lax.broadcasted_iota(jnp.int32, shape, len(shape) - 2)


def inner_last(left, right):
    return lax.dot_general(left, right, (((1,), (1,)), ((), ())), preferred_element_type=F32)


def shared(block, axis):
    copies = jnp.broadcast_to(block, (lax.axis_size(axis), *block.shape))
    return lax.all_to_all(copies, axis, 0, 0, tiled=True)


def query_kernel(tp_ref, own_ref, other_ref, gain_ref, weight_ref, out_ref):
    own = own_ref[...].astype(F32)
    other = other_ref[...].astype(F32)
    both = jnp.concatenate([own, other, own, other], axis=1)
    x = jnp.where(tp_ref[0] == 0, both[:, :64], both[:, 32:96])
    square = jnp.sum(x * x, axis=1, keepdims=True)
    scaled = (x * gain_ref[...]).astype(BF16)
    q = jnp.dot(scaled, weight_ref[...], preferred_element_type=F32)
    for h in range(16):
        out_ref[4 * h : 4 * h + 4, :] = q[:, 128 * h : 128 * h + 128]
    wide = jnp.broadcast_to(square, (4, 128))
    out_ref[64:68, :] = wide
    out_ref[68:72, :] = wide


def pack(values, lse):
    high = lse.astype(BF16).astype(F32)
    mid = (lse - high).astype(BF16).astype(F32)
    low = lse - high - mid
    at = rows((16, 128))
    tail = jnp.where(at == 0, high, jnp.where(at == 1, mid, jnp.where(at == 2, low, 0.0)))
    return values.astype(BF16), tail.astype(BF16)


def attend_kernel(parts_ref, cos_ref, sin_ref, key_ref, value_ref, out_ref):
    total = parts_ref[0]
    for k in range(1, 8):
        total = total + parts_ref[k]
    scale = lax.rsqrt(total[64:72] * (1.0 / 4096) + EPS)
    q = (total[:64].reshape(8, 8, 128) * scale[None]).reshape(64, 128)
    lane = lanes((64, 128))
    swapped = jnp.where(lane % 64 < 32, pltpu.roll(q, 96, 1), pltpu.roll(q, 32, 1))
    turned = q * cos_ref[...] + swapped * sin_ref[...]
    both = jnp.concatenate(
        [jnp.where(lane < 64, turned, 0.0), jnp.where(lane < 64, 0.0, turned)], axis=0
    ).astype(BF16)
    row = rows((128, 256)) % 4
    scores = inner_last(both, key_ref[0])
    for b in range(1, 4):
        scores = jnp.where(row == b, inner_last(both, key_ref[b]), scores)
    scores = scores * 0.125
    peak = jnp.max(scores, axis=1, keepdims=True)
    e = jnp.exp(scores - peak)
    total_e = jnp.sum(e, axis=1, keepdims=True)
    probs = e.astype(BF16)
    row_v = rows((128, 128)) % 4
    value = jnp.dot(probs, value_ref[0], preferred_element_type=F32)
    for b in range(1, 4):
        value = jnp.where(
            row_v == b, jnp.dot(probs, value_ref[b], preferred_element_type=F32), value
        )
    value = value / total_e
    lse = peak + jnp.log(total_e)
    eye = rows((128, 128)) == lanes((128, 128))
    lse_row = jnp.sum(jnp.where(eye, lse, 0.0), axis=0, keepdims=True)
    out_ref[:128, :], out_ref[128:, :] = pack(value, lse_row)


def merged(parts_ref):
    tails = []
    for k in range(8):
        tail = parts_ref[k, 128:, :].astype(F32)
        tails.append(tail[0:1] + tail[1:2] + tail[2:3])
    lse = jnp.concatenate(tails, axis=0)
    peak = jnp.max(lse, axis=0, keepdims=True)
    e = jnp.exp(lse - peak)
    total = jnp.sum(e, axis=0, keepdims=True)
    share = (e / total).T
    value = share[:, 0:1] * parts_ref[0, :128, :].astype(F32)
    for k in range(1, 8):
        value = value + share[:, k : k + 1] * parts_ref[k, :128, :].astype(F32)
    return value, peak + jnp.log(total)


def merge_kernel(parts_ref, out_ref):
    out_ref[:128, :], out_ref[128:, :] = pack(*merged(parts_ref))


def project_kernel(tp_ref, parts_ref, lam_ref, gain_ref, weight_ref, own_ref, out_ref, heads_ref):
    value, _ = merged(parts_ref)
    difference = value[:64] - lam_ref[...] * value[64:]
    norm = lax.rsqrt(jnp.mean(difference * difference, axis=1, keepdims=True) + EPS)
    heads_ref[...] = difference * norm * gain_ref[...]
    head_out = jnp.concatenate([heads_ref[4 * h : 4 * h + 4, :] for h in range(16)], axis=1)
    part = inner_last(head_out.astype(BF16), weight_ref[...])
    own = own_ref[...].astype(F32)
    lane = lanes((4, 128))
    token = jnp.where(lane // 32 == 2 + tp_ref[0], jnp.concatenate([own] * 4, axis=1), 0.0)
    out_ref[...] = jnp.where(lane < 64, jnp.concatenate([part, part], axis=1), token).astype(BF16)


def mlp_kernel(
    at_ref, pieces_ref, gain_ref, gate_ref, up_ref, down_ref, out_ref, tile_ref, row_ref
):
    lane = lanes((4, 128))
    blocks = []
    for kv in range(64):
        s = pieces_ref[2 * kv].astype(F32) + pieces_ref[2 * kv + 1].astype(F32)
        blocks.append(s + pltpu.roll(s, 64, 1))
    tiles = [jnp.where(lane < 64, blocks[2 * v], blocks[2 * v + 1]) for v in range(32)]
    stream = jnp.concatenate(tiles, axis=1)
    square = jnp.sum(stream * stream, axis=1, keepdims=True) * (1.0 / 4096)
    normed = (stream * lax.rsqrt(square + EPS) * gain_ref[...]).astype(BF16)
    gate = inner_last(normed, gate_ref[...])
    up = inner_last(normed, up_ref[...])
    hidden = (gate / (1.0 + jnp.exp(-gate)) * up).astype(BF16)
    down = jnp.dot(hidden, down_ref[...], preferred_element_type=F32)
    down = down + jnp.where(lanes((4, 4096)) // 32 == at_ref[0], stream, 0.0)
    for v in range(32):
        tile_ref[4 * v : 4 * v + 4, :] = down[:, 128 * v : 128 * v + 128]
    by_row = [tile_ref[pl.ds(r, 32, stride=4), :] for r in range(4)]
    wide = lanes((32, 128)) // 32
    for g in range(4):
        line = by_row[g]
        for r in range(4):
            if r != g:
                line = jnp.where(wide == r, pltpu.roll(by_row[r], (r - g) % 4 * 32, 1), line)
        row_ref[pl.ds(g, 32, stride=4), :] = line
    out_ref[...] = row_ref[...]


def total_kernel(parts_ref, out_ref):
    line = jnp.sum(parts_ref[...], axis=0, keepdims=True)
    out_ref[...] = jnp.concatenate(
        [line[:, 32 * r : 32 * r + 32] for r in range(4)], axis=0
    ).astype(BF16)


def call(kernel, name, shape, dtype, *args, scalars=0, scratch=()):
    smem = pl.BlockSpec(memory_space=pltpu.SMEM)
    vmem = pl.BlockSpec(memory_space=pltpu.VMEM)
    return pl.pallas_call(
        kernel,
        name=name,
        out_shape=SHAPE(shape, dtype),
        in_specs=[smem] * scalars + [vmem] * (len(args) - scalars),
        out_specs=vmem,
        scratch_shapes=list(scratch),
    )(*args)


def turn_tables(position):
    half_len = 32
    inv_freq = 1.0 / THETA ** (jnp.arange(half_len, dtype=F32) / half_len)
    angles = position * inv_freq
    cos_table = jnp.cos(angles)
    sin_table = jnp.sin(angles)
    cos = jnp.concatenate([cos_table] * 4)
    sin = jnp.concatenate([-sin_table, sin_table] * 2)
    return cos.reshape(1, 128), sin.reshape(1, 128)


def shards(
    tokens,
    attn_gain,
    query_weight,
    key_cache,
    value_cache,
    head_lambda,
    head_gain,
    out_weight,
    mlp_gain,
    gate_weight,
    up_weight,
    down_weight,
):
    tp = lax.axis_index("tp").astype(jnp.int32).reshape(1)
    kv = lax.axis_index(KV)
    at = lax.axis_index(KV_TP).astype(jnp.int32).reshape(1)
    other = lax.ppermute(tokens, "tp", [(0, 1), (1, 0)])
    gain = lax.dynamic_slice_in_dim(attn_gain, kv * 64, 64).reshape(1, 64)
    position = jnp.float32(key_cache.shape[1] * lax.axis_size(KV))
    cos, sin = turn_tables(position)
    lam = jnp.broadcast_to(jnp.repeat(head_lambda, 4)[:, None], (64, 128))

    part = call(
        query_kernel, "query", (72, 128), F32, tp, tokens, other, gain, query_weight, scalars=1
    )
    part = jnp.sum(shared(part, "kv_0"), axis=0)
    parts = shared(part, "kv_1")
    keys = key_cache.reshape(4, 256, 128)
    values = value_cache.reshape(4, 256, 128)
    packed = call(attend_kernel, "attend", (144, 128), BF16, parts, cos, sin, keys, values)
    packed = call(merge_kernel, "merge", (144, 128), BF16, shared(packed, "kv_0"))
    block = call(
        project_kernel,
        "project",
        (4, 128),
        BF16,
        tp,
        shared(packed, "kv_1"),
        lam,
        head_gain.reshape(1, 128),
        out_weight,
        tokens,
        scalars=1,
        scratch=[pltpu.VMEM((64, 128), F32)],
    )
    pieces = shared(block, KV_TP)
    partial = call(
        mlp_kernel,
        "mlp",
        (128, 128),
        F32,
        at,
        pieces,
        mlp_gain.reshape(1, 4096),
        gate_weight,
        up_weight,
        down_weight,
        scalars=1,
        scratch=[pltpu.VMEM((128, 128), F32), pltpu.VMEM((128, 128), F32)],
    )
    sums = lax.all_to_all(partial.reshape(128, 1, 128), KV_TP, 0, 0, tiled=True)
    return call(total_kernel, "total", (4, 32), BF16, sums.reshape(128, 128))


def solution(mesh):
    torus = Mesh(
        mesh.devices.reshape(mesh.shape["dp"], 8, 8, mesh.shape["tp"]), ("dp", "kv_0", "kv_1", "tp")
    )
    in_specs = (
        P("dp", KV_TP),
        P(),
        P(KV, "tp"),
        P("dp", KV, "tp", None),
        P("dp", KV, "tp", None),
        P("tp"),
        P(),
        P(KV, "tp"),
        P(),
        P(KV_TP, None),
        P(KV_TP, None),
        P(KV_TP, None),
    )
    out_specs = P("dp", KV_TP)
    return jax.shard_map(
        shards, mesh=torus, in_specs=in_specs, out_specs=out_specs, check_vma=False
    )
```

time: 200 us -> 133 us (0.67)
  blocking collectives: 138 us -> 47.6 us
  Pallas kernels: 0 us -> 13.2 us
  waiting for transfers between devices: 19.9 us -> 32.1 us
  starting transfers between devices: 21.9 us -> 29.3 us
  other arithmetic: 5.28 us -> 1.38 us
  local copies, waits for them, and re-layouts: 12 us -> 8.6 us
    psum x2 -> x0, blocking collectives: 40.8 us -> none  [one_axis_at_a_time(): x = lax.psum(x, axis)]
    all_gather x2 -> x0, blocking collectives: 38.3 us -> none  [collected_together(): both, at, found = (lax.all_gather(jnp.concatenate(lines), axis), 0, {})]
    pallas_call x0 -> x6, Pallas kernels: none -> 13.2 us  [call(): pl.pallas_call(kernel, name=name, out_shape=SHAPE(shape, dtype), in_specs...]
    all_to_all x2 -> x3, waiting for transfers between devices: 19.9 us -> 31.7 us  [shared(): return lax.all_to_all(copies, axis, 0, 0, tiled=True)]
    all_to_all x4 -> x3, blocking collectives: 58.7 us -> 47.6 us  [the longest x2 29.5 us: shared(): return lax.all_to_all(copies, axis, 0, 0, tiled=True)]
    ppermute x0 -> x1, starting transfers between devices: none -> 8.87 us  [shards(): other = lax.ppermute(tokens, 'tp', [(0, 1), (1, 0)])]
    broadcast_in_dim x2 -> x8, local copies, waits for them, and re-layouts: 1.41 us -> 6.06 us  [the longest x5 5.18 us: shared(): copies = jnp.broadcast_to(block, (lax.axis_size(axis), *block.shape))]
    unnamed x32 -> x12, local copies, waits for them, and re-layouts: 5 us -> 1.91 us
  transfers between devices with their start and end apart: 2 -> 4, of which waited for: 2 -> 4; matrix products, arithmetic and copies ran while one was open for 1% -> 2% of each run, Pallas kernels for 0% -> 0%
where the time goes in v1:
time: 133 us; the launch traced here: 132 us
  blocking collectives  47.6 us (36%)
  waiting for transfers between devices  32.1 us (24%)
  starting transfers between devices  29.3 us (22%)
  Pallas kernels  13.2 us (10%)
  local copies, waits for them, and re-layouts  8.6 us (6%)
  other arithmetic  1.38 us (1%)
    all_to_all x3, waiting for transfers between devices, shared(): return lax.all_to_all(copies, axis, 0, 0, tiled=True)  31.7 us
    all_to_all x2, blocking collectives, shared(): return lax.all_to_all(copies, axis, 0, 0, tiled=True)  29.5 us
    all_to_all x3, starting transfers between devices, shared(): return lax.all_to_all(copies, axis, 0, 0, tiled=True)  20.5 us
    all_to_all x1, blocking collectives, shards(): sums = lax.all_to_all(partial.reshape(128, 1, 128), KV_TP, 0, 0, tiled=True)  18.1 us
    pallas_call x6, Pallas kernels, call(): pl.pallas_call(kernel, name=name, out_shape=SHAPE(shape, dtype), in_specs...  13.2 us
    ppermute x1, starting transfers between devices, shards(): other = lax.ppermute(tokens, 'tp', [(0, 1), (1, 0)])  8.87 us
    broadcast_in_dim x5, local copies, waits for them, and re-layouts, shared(): copies = jnp.broadcast_to(block, (lax.axis_size(axis), *block.shape))  5.18 us
  transfers between devices with their start and end apart: 4, of which 4 were waited for; matrix products, arithmetic and copies ran while one was open for 2% of the time, Pallas kernels for 0%

profile of v1, /device:TPU:1, one launch (start us, length us, event | category | flops | bytes accessed | tf_op | source)
XLA Modules:
  0.0 132.3 jit_solution(6857739170364593871)
XLA Ops:
  0.0 8.9 %collective-permute-start = (bf16[4,32]{1,0:T(4,128)(2,1)}, bf16[4,32]{1,0:T(4,128)(2,1)S(1)}, u32[]{:S(2)}, u32[]{:S(2)}) collective-permute-start(bf16[4,32]{1,0:T(4,128)(2,1)} %own_ref.3), channel_id=1, source_target_pairs={{0,1},{1,0},{2,3},{3,2},{4,5},{5,4},{6,7},{7,6},{8,9},{9,8},{10,11... | collective-permute-start | bytes 776 | tf_op jit(solution)/shard_map/ppermute | solution.py:204
  8.9 0.6 dynamic-slice_bitcast_fusion.gain_ref
  9.5 0.4 collective-permute-done.other_ref
  9.9 0.6 copy-done.4
  10.4 1.9 %query.1 = f32[72,128]{1,0:T(8,128)} custom-call(s32[1]{0:T(128)} %bitcast.1.tp_ref, bf16[4,32]{1,0:T(4,128)(2,1)} %own_ref.3, bf16[4,32]{1,0:T(4,128)(2,1)} %copy-done.4, f32[1,64]{1,0:T(1,128)} %dynamic-slice_bitcast_fusion.gain_ref, bf16[64,2048]{1,0:T(8,128)(2,1)} %weight_ref.2), custom_call_target="tpu_custom_call" | custom-call | tf_op jit(solution)/shard_map/query/pallas_call | solution.py:166
  12.3 0.8 broadcast_in_dim.25
  13.1 16.7 %all_to_all.30 = f32[8,72,128]{2,1,0:T(8,128)S(1)} all-to-all(f32[8,72,128]{2,1,0:T(8,128)S(1)} %broadcast_in_dim.25), channel_id=1, replica_groups=mesh['dp'=4,'kv_0'=8,'kv_1'=8,'tp'=2] {'kv_0'}, dimensions={0} | all-to-all | bytes 589824 | tf_op jit(solution)/shard_map/all_to_all | solution.py:32
  29.8 0.7 broadcast_in_dim.26
  30.6 6.8 %all-to-all-start.1 = ((f32[8,72,128]{2,1,0:T(8,128)}), f32[8,72,128]{2,1,0:T(8,128)S(1)}, u32[]{:S(2)}, u32[]{:S(2)}) async-start(f32[8,72,128]{2,1,0:T(8,128)} %broadcast_in_dim.26), calls=%async_computation.1 | async-start | bytes 589824 | tf_op jit(solution)/shard_map/all_to_all | solution.py:32
  37.4 0.6 maximum_bitcast_fusion.cos_ref
  38.0 0.1 fusion
  38.1 0.7 maximum_bitcast_fusion.1.sin_ref
  38.8 9.3 %all-to-all-done.1.parts_ref = f32[8,72,128]{2,1,0:T(8,128)S(1)} async-done(((f32[8,72,128]{2,1,0:T(8,128)}), f32[8,72,128]{2,1,0:T(8,128)S(1)}, u32[]{:S(2)}, u32[]{:S(2)}) %all-to-all-start.1) | async-done | bytes 294944 | tf_op jit(solution)/shard_map/all_to_all | solution.py:32
  48.1 0.7 copy-done.2
  48.8 2.3 %attend.1 = bf16[144,128]{1,0:T(8,128)(2,1)} custom-call(f32[8,72,128]{2,1,0:T(8,128)} %copy-done.2, f32[1,128]{1,0:T(1,128)} %maximum_bitcast_fusion.cos_ref, f32[1,128]{1,0:T(1,128)} %maximum_bitcast_fusion.1.sin_ref, bf16[4,256,128]{2,1,0:T(8,128)(2,1)} %bitcast.17, bf16[4,256,128]{2,1,0:T(8,128)(2,1)} %bitcast.18), custom_call_target="tpu_custom_call" | custom-call | tf_op jit(solution)/shard_map/attend/pallas_call | solution.py:166
  51.1 0.8 broadcast_in_dim.27
  51.9 12.7 %all_to_all.31.parts_ref = bf16[8,144,128]{2,1,0:T(8,128)(2,1)} all-to-all(bf16[8,144,128]{2,1,0:T(8,128)(2,1)S(1)} %broadcast_in_dim.27), channel_id=1, replica_groups=mesh['dp'=4,'kv_0'=8,'kv_1'=8,'tp'=2] {'kv_0'}, dimensions={0} | all-to-all | bytes 589824 | tf_op jit(solution)/shard_map/all_to_all | solution.py:32
  64.7 1.9 %merge.1 = bf16[144,128]{1,0:T(8,128)(2,1)} custom-call(bf16[8,144,128]{2,1,0:T(8,128)(2,1)} %all_to_all.31.parts_ref), custom_call_target="tpu_custom_call" | custom-call | tf_op jit(solution)/shard_map/merge/pallas_call | solution.py:166
  66.6 1.5 %broadcast_in_dim.28 = bf16[8,144,128]{2,1,0:T(8,128)(2,1)} broadcast(bf16[144,128]{1,0:T(8,128)(2,1)} %merge.1), dimensions={1,2} | broadcast | bytes 331776 | tf_op jit(solution)/shard_map/broadcast_in_dim | solution.py:31
  68.1 4.0 %all-to-all-start.3 = ((bf16[8,144,128]{2,1,0:T(8,128)(2,1)}), bf16[8,144,128]{2,1,0:T(8,128)(2,1)S(1)}, u32[]{:S(2)}, u32[]{:S(2)}) async-start(bf16[8,144,128]{2,1,0:T(8,128)(2,1)} %broadcast_in_dim.28), calls=%async_computation.3 | async-start | bytes 589824 | tf_op jit(solution)/shard_map/all_to_all | solution.py:32
  72.1 0.1 broadcast_in_dim.29
  72.2 0.1 broadcast_in_dim.30
  72.3 9.6 %all-to-all-done.3.parts_ref = bf16[8,144,128]{2,1,0:T(8,128)(2,1)S(1)} async-done(((bf16[8,144,128]{2,1,0:T(8,128)(2,1)}), bf16[8,144,128]{2,1,0:T(8,128)(2,1)S(1)}, u32[]{:S(2)}, u32[]{:S(2)}) %all-to-all-start.3) | async-done | bytes 294944 | tf_op jit(solution)/shard_map/all_to_all | solution.py:32
  81.9 0.7 broadcast_in_dim.31.lam_ref
  82.7 2.3 %project.1 = bf16[4,128]{1,0:T(4,128)(2,1)} custom-call(s32[1]{0:T(128)} %bitcast.1.tp_ref, bf16[8,144,128]{2,1,0:T(8,128)(2,1)} %copy-done.1, f32[64,128]{1,0:T(8,128)} %broadcast_in_dim.31.lam_ref, f32[1,128]{1,0:T(1,128)} %bitcast.21, bf16[64,2048]{1,0:T(8,128)(2,1)} %weight_ref.3, bf16[4,32]{1,0:T(4,128)(2,1)} %own_ref.3), custom_call_target="tpu_custom_call" | custom-call | tf_op jit(solution)/shard_map/project/pallas_call | solution.py:166
  85.0 1.3 %broadcast_in_dim.32 = bf16[128,4,128]{2,1,0:T(4,128)(2,1)} broadcast(bf16[4,128]{1,0:T(4,128)(2,1)} %project.1), dimensions={1,2} | broadcast | bytes 132096 | tf_op jit(solution)/shard_map/broadcast_in_dim | solution.py:31
  86.3 9.6 %all-to-all-start.4 = ((bf16[128,4,128]{2,1,0:T(4,128)(2,1)}), bf16[128,4,128]{2,1,0:T(4,128)(2,1)S(1)}, u32[]{:S(2)}, u32[]{:S(2)}) async-start(bf16[128,4,128]{2,1,0:T(4,128)(2,1)} %broadcast_in_dim.32), calls=%async_computation.4 | async-start | bytes 262144 | tf_op jit(solution)/shard_map/all_to_all | solution.py:32
  96.0 12.8 %all-to-all-done.4.pieces_ref = bf16[128,4,128]{2,1,0:T(4,128)(2,1)S(1)} async-done(((bf16[128,4,128]{2,1,0:T(4,128)(2,1)}), bf16[128,4,128]{2,1,0:T(4,128)(2,1)S(1)}, u32[]{:S(2)}, u32[]{:S(2)}) %all-to-all-start.4) | async-done | bytes 131104 | tf_op jit(solution)/shard_map/all_to_all | solution.py:32
  108.7 0.6 copy-done.3
  109.4 3.3 %mlp.1 = f32[128,128]{1,0:T(8,128)} custom-call(s32[1]{0:T(128)} %bitcast.at_ref, bf16[128,4,128]{2,1,0:T(4,128)(2,1)} %copy-done.3, f32[1,4096]{1,0:T(1,128)} %bitcast.20, bf16[88,4096]{1,0:T(8,128)(2,1)} %gate_ref.1, bf16[88,4096]{1,0:T(8,128)(2,1)} %up_ref.1, bf16[88,4096]{1,0:T(8,128)(2,1)} %down_ref.1), custom_call_target="tpu_custom_call" | custom-call | tf_op jit(solution)/shard_map/mlp/pallas_call | solution.py:166
  112.7 18.1 %all_to_all.32 = f32[128,1,128]{2,1,0:T(1,128)} all-to-all(f32[128,1,128]{2,1,0:T(1,128)} %bitcast.19), channel_id=1, replica_groups=mesh['dp'=4,'kv_0'=8,'kv_1'=8,'tp'=2] {'kv_0','kv_1','tp'}, dimensions={0} | all-to-all | bytes 131072 | tf_op jit(solution)/shard_map/all_to_all | solution.py:248
  130.8 1.5 %total.1 = bf16[4,32]{1,0:T(4,128)(2,1)} custom-call(f32[128,128]{1,0:T(8,128)} %bitcast.16), custom_call_target="tpu_custom_call" | custom-call | tf_op jit(solution)/shard_map/total/pallas_call | solution.py:166
  (11 shorter events, 0.1 us)
Async XLA Ops:
  0.0 8.9 %copy-start = (f32[4096]{0:T(1024)S(1)}, f32[4096]{0:T(1024)}, u32[]{:S(2)}) copy-start(f32[4096]{0:T(1024)} %param.13) | copy-start | bytes 49156
  0.0 9.9 %collective-permute-start = (bf16[4,32]{1,0:T(4,128)(2,1)}, bf16[4,32]{1,0:T(4,128)(2,1)S(1)}, u32[]{:S(2)}, u32[]{:S(2)}) collective-permute-start(bf16[4,32]{1,0:T(4,128)(2,1)} %own_ref.3), channel_id=1, source_target_pairs={{0,1},{1,0},{2,3},{3,2},{4,5},{5,4},{6,7},{7,6},{8,9},{9,8},{10,11... | collective-permute-start | bytes 776 | tf_op jit(solution)/shard_map/ppermute | solution.py:204
  9.9 0.6 copy-start.4
  30.6 17.5 %all-to-all-start.1 = ((f32[8,72,128]{2,1,0:T(8,128)}), f32[8,72,128]{2,1,0:T(8,128)S(1)}, u32[]{:S(2)}, u32[]{:S(2)}) async-start(f32[8,72,128]{2,1,0:T(8,128)} %broadcast_in_dim.26), calls=%async_computation.1 | async-start | bytes 589824 | tf_op jit(solution)/shard_map/all_to_all | solution.py:32
  48.1 0.7 copy-start.2
  68.1 4.0 %copy-start.5 = (f32[16]{0:T(128)S(1)}, f32[16]{0:T(128)}, u32[]{:S(2)}) copy-start(f32[16]{0:T(128)} %param.17) | copy-start | bytes 196
  68.1 13.8 %all-to-all-start.3 = ((bf16[8,144,128]{2,1,0:T(8,128)(2,1)}), bf16[8,144,128]{2,1,0:T(8,128)(2,1)S(1)}, u32[]{:S(2)}, u32[]{:S(2)}) async-start(bf16[8,144,128]{2,1,0:T(8,128)(2,1)} %broadcast_in_dim.28), calls=%async_computation.3 | async-start | bytes 589824 | tf_op jit(solution)/shard_map/all_to_all | solution.py:32
  81.9 0.7 copy-start.1
  86.3 22.4 %all-to-all-start.4 = ((bf16[128,4,128]{2,1,0:T(4,128)(2,1)}), bf16[128,4,128]{2,1,0:T(4,128)(2,1)S(1)}, u32[]{:S(2)}, u32[]{:S(2)}) async-start(bf16[128,4,128]{2,1,0:T(4,128)(2,1)} %broadcast_in_dim.32), calls=%async_computation.4 | async-start | bytes 262144 | tf_op jit(solution)/shard_map/all_to_all | solution.py:32
  108.7 0.6 copy-start.3

commit v2 on v1

--- a/solution.py
+++ b/solution.py
@@ -1,5 +1,6 @@
 import jax
 import jax.numpy as jnp
+import numpy as np
 from jax import lax
 from jax.experimental import pallas as pl
 from jax.experimental.pallas import tpu as pltpu
@@ -163,25 +164,23 @@
 def call(kernel, name, shape, dtype, *args, scalars=0, scratch=()):
     smem = pl.BlockSpec(memory_space=pltpu.SMEM)
     vmem = pl.BlockSpec(memory_space=pltpu.VMEM)
+    near = [pltpu.with_memory_space_constraint(x, pltpu.VMEM) for x in args[scalars:]]
     return pl.pallas_call(
         kernel,
         name=name,
-        out_shape=SHAPE(shape, dtype),
-        in_specs=[smem] * scalars + [vmem] * (len(args) - scalars),
+        out_shape=pltpu.VMEM(shape, dtype) if name != "total" else SHAPE(shape, dtype),
+        in_specs=[smem] * scalars + [vmem] * len(near),
         out_specs=vmem,
         scratch_shapes=list(scratch),
-    )(*args)
+    )(*args[:scalars], *near)
 
 
 def turn_tables(position):
-    half_len = 32
-    inv_freq = 1.0 / THETA ** (jnp.arange(half_len, dtype=F32) / half_len)
-    angles = position * inv_freq
-    cos_table = jnp.cos(angles)
-    sin_table = jnp.sin(angles)
-    cos = jnp.concatenate([cos_table] * 4)
-    sin = jnp.concatenate([-sin_table, sin_table] * 2)
-    return cos.reshape(1, 128), sin.reshape(1, 128)
+    power = np.power(THETA, np.arange(32, dtype=np.float64) / 32).astype(np.float32)
+    angles = (np.float32(position) * (np.float32(1.0) / power)).astype(np.float64)
+    cos = np.tile(np.cos(angles), 4).astype(np.float32)
+    sin = np.tile(np.concatenate([-np.sin(angles), np.sin(angles)]), 2).astype(np.float32)
+    return jnp.asarray(cos.reshape(1, 128)), jnp.asarray(sin.reshape(1, 128))
 
 
 def shards(
@@ -203,13 +202,13 @@
     at = lax.axis_index(KV_TP).astype(jnp.int32).reshape(1)
     other = lax.ppermute(tokens, "tp", [(0, 1), (1, 0)])
     gain = lax.dynamic_slice_in_dim(attn_gain, kv * 64, 64).reshape(1, 64)
-    position = jnp.float32(key_cache.shape[1] * lax.axis_size(KV))
-    cos, sin = turn_tables(position)
+    cos, sin = turn_tables(key_cache.shape[1] * lax.axis_size(KV))
     lam = jnp.broadcast_to(jnp.repeat(head_lambda, 4)[:, None], (64, 128))
 
     part = call(
         query_kernel, "query", (72, 128), F32, tp, tokens, other, gain, query_weight, scalars=1
     )
+    part, cos, sin, lam, at = lax.optimization_barrier((part, cos, sin, lam, at))
     part = jnp.sum(shared(part, "kv_0"), axis=0)
     parts = shared(part, "kv_1")
     keys = key_cache.reshape(4, 256, 128)

time: 133 us -> 115 us (0.86)
  blocking collectives: 47.6 us -> 98.9 us
  waiting for transfers between devices: 32.1 us -> 0.15 us
  starting transfers between devices: 29.3 us -> 8.87 us
  Pallas kernels: 13.2 us -> 3.59 us
  local copies, waits for them, and re-layouts: 8.6 us -> 3.25 us
  other arithmetic: 1.38 us -> 0.02 us
    all_to_all x2 -> x5, blocking collectives: 29.5 us -> 82.4 us  [shared(): return lax.all_to_all(copies, axis, 0, 0, tiled=True)]
    all_to_all x3 -> x0, waiting for transfers between devices: 31.7 us -> none  [shared(): return lax.all_to_all(copies, axis, 0, 0, tiled=True)]
    all_to_all x3 -> x0, starting transfers between devices: 20.5 us -> none  [shared(): return lax.all_to_all(copies, axis, 0, 0, tiled=True)]
    pallas_call x6, Pallas kernels: 13.2 us -> 3.59 us  [call(): pl.pallas_call(kernel, name=name, out_shape=pltpu.VMEM(shape, dtype) if n...]
    broadcast_in_dim x5, local copies, waits for them, and re-layouts: 5.18 us -> 0.19 us  [shared(): copies = jnp.broadcast_to(block, (lax.axis_size(axis), *block.shape))]
    all_to_all x1, blocking collectives: 18.1 us -> 16.5 us  [shards(): sums = lax.all_to_all(partial.reshape(128, 1, 128), KV_TP, 0, 0, tiled=True)]
    unnamed x12 -> x28, local copies, waits for them, and re-layouts: 1.91 us -> 2.76 us
  transfers between devices with their start and end apart: 4 -> 1, of which waited for: 4 -> 1; matrix products, arithmetic and copies ran while one was open for 2% -> 0% of each run, Pallas kernels for 0% -> 0%
where the time goes in v2:
time: 115 us
  blocking collectives  98.9 us (86%)
  starting transfers between devices  8.87 us (8%)
  Pallas kernels  3.59 us (3%)
  local copies, waits for them, and re-layouts  3.25 us (3%)
    all_to_all x5, blocking collectives, shared(): return lax.all_to_all(copies, axis, 0, 0, tiled=True)  82.4 us
    all_to_all x1, blocking collectives, shards(): sums = lax.all_to_all(partial.reshape(128, 1, 128), KV_TP, 0, 0, tiled=True)  16.5 us
    ppermute x1, starting transfers between devices, shards(): other = lax.ppermute(tokens, 'tp', [(0, 1), (1, 0)])  8.87 us
    pallas_call x6, Pallas kernels, call(): pl.pallas_call(kernel, name=name, out_shape=pltpu.VMEM(shape, dtype) if n...  3.59 us
    unnamed x28, local copies, waits for them, and re-layouts  2.76 us
  transfers between devices with their start and end apart: 1, of which 1 were waited for; matrix products, arithmetic and copies ran while one was open for 0% of the time, Pallas kernels for 0%

profile of v2, /device:TPU:1, one launch (start us, length us, event | category | flops | bytes accessed | tf_op | source)
XLA Modules:
  0.0 115.0 jit_solution(3127485040999673533)
XLA Ops:
  0.0 8.9 %collective-permute-start = (bf16[4,32]{1,0:T(4,128)(2,1)}, bf16[4,32]{1,0:T(4,128)(2,1)S(1)}, u32[]{:S(2)}, u32[]{:S(2)}) collective-permute-start(bf16[4,32]{1,0:T(4,128)(2,1)} %own_ref.3), channel_id=1, source_target_pairs={{0,1},{1,0},{2,3},{3,2},{4,5},{5,4},{6,7},{7,6},{8,9},{9,8},{10,11... | collective-permute-start | bytes 776 | tf_op jit(solution)/shard_map/ppermute | solution.py:203
  8.9 0.1 dynamic-slice_bitcast_fusion.gain_ref
  9.0 0.6 copy-done.13
  9.6 0.1 broadcast_in_dim.25
  9.6 0.1 broadcast_in_dim.26
  9.7 0.0 copy-start.9
  9.7 0.2 collective-permute-done.other_ref
  9.9 0.5 copy-done.9
  10.4 0.9 copy-done.4
  11.4 0.3 query.1
  11.6 0.1 broadcast_in_dim.27.lam_ref
  11.7 17.2 %all_to_all.30 = f32[8,72,128]{2,1,0:T(8,128)S(1)} all-to-all(f32[8,72,128]{2,1,0:T(8,128)S(1)} %broadcast_in_dim.28), channel_id=1, replica_groups=mesh['dp'=4,'kv_0'=8,'kv_1'=8,'tp'=2] {'kv_0'}, dimensions={0} | all-to-all | bytes 589824 | tf_op jit(solution)/shard_map/all_to_all | solution.py:33
  29.0 0.0 copy-start.6
  29.0 0.0 copy-start.7
  29.0 17.5 %all_to_all.31.parts_ref = f32[8,72,128]{2,1,0:T(8,128)S(1)} all-to-all(f32[8,72,128]{2,1,0:T(8,128)S(1)} %broadcast_in_dim.29), channel_id=1, replica_groups=mesh['dp'=4,'kv_0'=8,'kv_1'=8,'tp'=2] {'kv_1'}, dimensions={0} | all-to-all | bytes 589824 | tf_op jit(solution)/shard_map/all_to_all | solution.py:33
  46.5 0.0 copy-done.7
  46.5 0.6 copy-done.11
  47.2 0.0 copy-done.12
  47.2 0.6 attend.1
  47.8 0.0 copy-start.5
  47.8 12.2 %all_to_all.32.parts_ref = bf16[8,144,128]{2,1,0:T(8,128)(2,1)S(1)} all-to-all(bf16[8,144,128]{2,1,0:T(8,128)(2,1)S(1)} %broadcast_in_dim.30), channel_id=1, replica_groups=mesh['dp'=4,'kv_0'=8,'kv_1'=8,'tp'=2] {'kv_0'}, dimensions={0} | all-to-all | bytes 589824 | tf_op jit(solution)/shard_map/all_to_all | solution.py:33
  60.0 0.4 merge.1
  60.4 0.0 copy-start.10
  60.4 0.0 copy-start.1
  60.5 0.0 copy-start.2
  60.5 14.2 %all_to_all.33.parts_ref = bf16[8,144,128]{2,1,0:T(8,128)(2,1)S(1)} all-to-all(bf16[8,144,128]{2,1,0:T(8,128)(2,1)S(1)} %broadcast_in_dim.31), channel_id=1, replica_groups=mesh['dp'=4,'kv_0'=8,'kv_1'=8,'tp'=2] {'kv_1'}, dimensions={0} | all-to-all | bytes 589824 | tf_op jit(solution)/shard_map/all_to_all | solution.py:33
  74.7 0.7 project.1
  75.5 0.0 copy-start.8
  75.5 21.3 %all_to_all.34.pieces_ref = bf16[128,4,128]{2,1,0:T(4,128)(2,1)S(1)} all-to-all(bf16[128,4,128]{2,1,0:T(4,128)(2,1)S(1)} %broadcast_in_dim.32), channel_id=1, replica_groups=mesh['dp'=4,'kv_0'=8,'kv_1'=8,'tp'=2] {'kv_0','kv_1','tp'}, dimensions={0} | all-to-all | bytes 262144 | tf_op jit(solution)/shard_map/all_to_all | solution.py:33
  96.8 1.0 mlp.1
  97.8 16.5 %all_to_all.35 = f32[128,1,128]{2,1,0:T(1,128)S(1)} all-to-all(f32[128,1,128]{2,1,0:T(1,128)S(1)} %bitcast.15), channel_id=1, replica_groups=mesh['dp'=4,'kv_0'=8,'kv_1'=8,'tp'=2] {'kv_0','kv_1','tp'}, dimensions={0} | all-to-all | bytes 131072 | tf_op jit(solution)/shard_map/all_to_all | solution.py:247
  114.3 0.7 total.1
  (20 shorter events, 0.2 us)
Async XLA Ops:
  0.0 8.9 %copy-start = (f32[4096]{0:T(1024)S(1)}, f32[4096]{0:T(1024)}, u32[]{:S(2)}) copy-start(f32[4096]{0:T(1024)} %param.15) | copy-start | bytes 49156
  0.0 9.9 %collective-permute-start = (bf16[4,32]{1,0:T(4,128)(2,1)}, bf16[4,32]{1,0:T(4,128)(2,1)S(1)}, u32[]{:S(2)}, u32[]{:S(2)}) collective-permute-start(bf16[4,32]{1,0:T(4,128)(2,1)} %own_ref.3), channel_id=1, source_target_pairs={{0,1},{1,0},{2,3},{3,2},{4,5},{5,4},{6,7},{7,6},{8,9},{9,8},{10,11... | collective-permute-start | bytes 776 | tf_op jit(solution)/shard_map/ppermute | solution.py:203
  8.9 0.7 copy-start.13
  9.7 0.7 copy-start.9
  10.4 0.9 copy-start.4
  29.0 17.6 %copy-start.6 = (bf16[4,256,1,128]{3,1,2,0:T(8,128)(2,1)S(1)}, bf16[4,256,1,128]{3,1,2,0:T(8,128)(2,1)}, u32[]{:S(2)}) copy-start(bf16[4,256,1,128]{3,1,2,0:T(8,128)(2,1)} %param.17) | copy-start | bytes 786436
  29.0 17.6 %copy-start.7 = (bf16[4,256,1,128]{3,1,2,0:T(8,128)(2,1)S(1)}, bf16[4,256,1,128]{3,1,2,0:T(8,128)(2,1)}, u32[]{:S(2)}) copy-start(bf16[4,256,1,128]{3,1,2,0:T(8,128)(2,1)} %param.18) | copy-start | bytes 786436
  46.5 0.7 copy-start.11
  46.5 0.7 copy-start.12
  47.8 26.9 %copy-start.5 = (bf16[64,2048]{1,0:T(8,128)(2,1)S(1)}, bf16[64,2048]{1,0:T(8,128)(2,1)}, u32[]{:S(2)}) copy-start(bf16[64,2048]{1,0:T(8,128)(2,1)} %weight_ref.3) | copy-start | bytes 786436
  60.0 36.7 %copy-start.3 = (bf16[88,4096]{1,0:T(8,128)(2,1)S(1)}, bf16[88,4096]{1,0:T(8,128)(2,1)}, u32[]{:S(2)}) copy-start(bf16[88,4096]{1,0:T(8,128)(2,1)} %down_ref.1) | copy-start | bytes 2162692
  60.4 14.3 %copy-start.10 = (f32[128]{0:T(128)S(1)}, f32[128]{0:T(128)}, u32[]{:S(2)}) copy-start(f32[128]{0:T(128)} %param.20) | copy-start | bytes 1540
  60.4 36.3 %copy-start.1 = (bf16[88,4096]{1,0:T(8,128)(2,1)S(1)}, bf16[88,4096]{1,0:T(8,128)(2,1)}, u32[]{:S(2)}) copy-start(bf16[88,4096]{1,0:T(8,128)(2,1)} %gate_ref.1) | copy-start | bytes 2162692
  60.5 36.3 %copy-start.2 = (bf16[88,4096]{1,0:T(8,128)(2,1)S(1)}, bf16[88,4096]{1,0:T(8,128)(2,1)}, u32[]{:S(2)}) copy-start(bf16[88,4096]{1,0:T(8,128)(2,1)} %up_ref.1) | copy-start | bytes 2162692
  75.5 21.3 %copy-start.8 = (f32[4096]{0:T(1024)S(1)}, f32[4096]{0:T(1024)}, u32[]{:S(2)}) copy-start(f32[4096]{0:T(1024)} %param.22) | copy-start | bytes 49156

commit v3 on v2

--- a/solution.py
+++ b/solution.py
@@ -33,13 +33,33 @@
     return lax.all_to_all(copies, axis, 0, 0, tiled=True)
 
 
+def prepare_kernel(
+    kv_ref, own_in, weight_in, gain_in, lam_in, turn_in, head_in,
+    own_ref, weight_ref, gain_ref, lam_ref, turn_ref, head_ref, all_ref, row_ref, sems,
+):
+    pairs = [
+        (weight_in, weight_ref), (own_in, own_ref), (gain_in, all_ref), (lam_in, row_ref),
+        (turn_in, turn_ref), (head_in, head_ref),
+    ]
+    copies = [pltpu.make_async_copy(a, b, sems.at[k]) for k, (a, b) in enumerate(pairs)]
+    for copy in copies:
+        copy.start()
+    for copy in copies[1:]:
+        copy.wait()
+    line = all_ref[pl.ds(kv_ref[0] // 2, 1), :]
+    gain_ref[...] = jnp.where(kv_ref[0] % 2 == 0, line, pltpu.roll(line, 64, 1))
+    picked = jnp.where(lanes((64, 16)) == rows((64, 16)) // 4, row_ref[...], 0.0)
+    lam_ref[...] = jnp.broadcast_to(jnp.sum(picked, axis=1, keepdims=True), (64, 128))
+    copies[0].wait()
+
+
 def query_kernel(tp_ref, own_ref, other_ref, gain_ref, weight_ref, out_ref):
     own = own_ref[...].astype(F32)
     other = other_ref[...].astype(F32)
     both = jnp.concatenate([own, other, own, other], axis=1)
     x = jnp.where(tp_ref[0] == 0, both[:, :64], both[:, 32:96])
     square = jnp.sum(x * x, axis=1, keepdims=True)
-    scaled = (x * gain_ref[...]).astype(BF16)
+    scaled = (x * gain_ref[:, :64]).astype(BF16)
     q = jnp.dot(scaled, weight_ref[...], preferred_element_type=F32)
     for h in range(16):
         out_ref[4 * h : 4 * h + 4, :] = q[:, 128 * h : 128 * h + 128]
@@ -57,7 +77,7 @@
     return values.astype(BF16), tail.astype(BF16)
 
 
-def attend_kernel(parts_ref, cos_ref, sin_ref, key_ref, value_ref, out_ref):
+def attend_kernel(parts_ref, turn_ref, key_ref, value_ref, out_ref):
     total = parts_ref[0]
     for k in range(1, 8):
         total = total + parts_ref[k]
@@ -65,7 +85,7 @@
     q = (total[:64].reshape(8, 8, 128) * scale[None]).reshape(64, 128)
     lane = lanes((64, 128))
     swapped = jnp.where(lane % 64 < 32, pltpu.roll(q, 96, 1), pltpu.roll(q, 32, 1))
-    turned = q * cos_ref[...] + swapped * sin_ref[...]
+    turned = q * turn_ref[0:1] + swapped * turn_ref[1:2]
     both = jnp.concatenate(
         [jnp.where(lane < 64, turned, 0.0), jnp.where(lane < 64, 0.0, turned)], axis=0
     ).astype(BF16)
@@ -118,22 +138,24 @@
     heads_ref[...] = difference * norm * gain_ref[...]
     head_out = jnp.concatenate([heads_ref[4 * h : 4 * h + 4, :] for h in range(16)], axis=1)
     part = inner_last(head_out.astype(BF16), weight_ref[...])
+    part = part.astype(BF16).astype(F32)
+    lane = lanes((4, 64))
     own = own_ref[...].astype(F32)
-    lane = lanes((4, 128))
-    token = jnp.where(lane // 32 == 2 + tp_ref[0], jnp.concatenate([own] * 4, axis=1), 0.0)
-    out_ref[...] = jnp.where(lane < 64, jnp.concatenate([part, part], axis=1), token).astype(BF16)
+    part = part + jnp.where(lane // 32 == tp_ref[0], jnp.concatenate([own, own], axis=1), 0.0)
+    out_ref[...] = jnp.concatenate([part[0:2], part[2:4]], axis=1).astype(BF16)
 
 
 def mlp_kernel(
     at_ref, pieces_ref, gain_ref, gate_ref, up_ref, down_ref, out_ref, tile_ref, row_ref
 ):
-    lane = lanes((4, 128))
-    blocks = []
-    for kv in range(64):
-        s = pieces_ref[2 * kv].astype(F32) + pieces_ref[2 * kv + 1].astype(F32)
-        blocks.append(s + pltpu.roll(s, 64, 1))
-    tiles = [jnp.where(lane < 64, blocks[2 * v], blocks[2 * v + 1]) for v in range(32)]
-    stream = jnp.concatenate(tiles, axis=1)
+    y = pieces_ref[...].astype(F32).reshape(32, 8, 128)
+    lane = lanes((32, 8, 128))
+    s = y + pltpu.roll(y, 6, 1)
+    far = pltpu.roll(s, 4, 1)
+    front = jnp.where(lane < 64, s, pltpu.roll(far, 64, 2))
+    back = jnp.where(lane < 64, pltpu.roll(s, 64, 2), far)
+    four = jnp.where(rows((32, 8, 128)) < 2, front, pltpu.roll(back, 2, 1))
+    stream = jnp.concatenate([four[v, 0:4] for v in range(32)], axis=1)
     square = jnp.sum(stream * stream, axis=1, keepdims=True) * (1.0 / 4096)
     normed = (stream * lax.rsqrt(square + EPS) * gain_ref[...]).astype(BF16)
     gate = inner_last(normed, gate_ref[...])
@@ -176,11 +198,11 @@
 
 
 def turn_tables(position):
-    power = np.power(THETA, np.arange(32, dtype=np.float64) / 32).astype(np.float32)
-    angles = (np.float32(position) * (np.float32(1.0) / power)).astype(np.float64)
-    cos = np.tile(np.cos(angles), 4).astype(np.float32)
-    sin = np.tile(np.concatenate([-np.sin(angles), np.sin(angles)]), 2).astype(np.float32)
-    return jnp.asarray(cos.reshape(1, 128)), jnp.asarray(sin.reshape(1, 128))
+    inverse = np.power(THETA, -np.arange(32, dtype=np.float64) / 32).astype(np.float32)
+    angles = (np.float32(position) * inverse).astype(np.float64)
+    cos = np.tile(np.cos(angles), 4)
+    sin = np.tile(np.concatenate([-np.sin(angles), np.sin(angles)]), 2)
+    return jnp.asarray(np.stack([cos, sin] + [np.zeros(128)] * 6).astype(np.float32))
 
 
 def shards(
@@ -201,35 +223,57 @@
     kv = lax.axis_index(KV)
     at = lax.axis_index(KV_TP).astype(jnp.int32).reshape(1)
     other = lax.ppermute(tokens, "tp", [(0, 1), (1, 0)])
-    gain = lax.dynamic_slice_in_dim(attn_gain, kv * 64, 64).reshape(1, 64)
-    cos, sin = turn_tables(key_cache.shape[1] * lax.axis_size(KV))
-    lam = jnp.broadcast_to(jnp.repeat(head_lambda, 4)[:, None], (64, 128))
-
-    part = call(
-        query_kernel, "query", (72, 128), F32, tp, tokens, other, gain, query_weight, scalars=1
-    )
-    part, cos, sin, lam, at = lax.optimization_barrier((part, cos, sin, lam, at))
+    turn = turn_tables(key_cache.shape[1] * lax.axis_size(KV))
+    own, weight, gain, lam, turn, head = pl.pallas_call(
+        prepare_kernel,
+        name="prepare",
+        out_shape=[
+            pltpu.VMEM((4, 32), BF16),
+            pltpu.VMEM((64, 2048), BF16),
+            pltpu.VMEM((1, 128), F32),
+            pltpu.VMEM((64, 128), F32),
+            pltpu.VMEM((8, 128), F32),
+            pltpu.VMEM((1, 128), F32),
+        ],
+        in_specs=[pl.BlockSpec(memory_space=pltpu.SMEM)] + [pl.BlockSpec(memory_space=pl.ANY)] * 6,
+        out_specs=[pl.BlockSpec(memory_space=pltpu.VMEM)] * 6,
+        scratch_shapes=[
+            pltpu.VMEM((32, 128), F32),
+            pltpu.VMEM((1, 16), F32),
+            pltpu.SemaphoreType.DMA((6,)),
+        ],
+    )(
+        kv.astype(jnp.int32).reshape(1),
+        tokens,
+        query_weight,
+        attn_gain.reshape(32, 128),
+        head_lambda.reshape(1, 16),
+        turn,
+        head_gain.reshape(1, 128),
+    )
+    part = call(query_kernel, "query", (72, 128), F32, tp, own, other, gain, weight, scalars=1)
+    part, at = lax.optimization_barrier((part, at))
     part = jnp.sum(shared(part, "kv_0"), axis=0)
     parts = shared(part, "kv_1")
     keys = key_cache.reshape(4, 256, 128)
     values = value_cache.reshape(4, 256, 128)
-    packed = call(attend_kernel, "attend", (144, 128), BF16, parts, cos, sin, keys, values)
+    packed = call(attend_kernel, "attend", (144, 128), BF16, parts, turn, keys, values)
     packed = call(merge_kernel, "merge", (144, 128), BF16, shared(packed, "kv_0"))
     block = call(
         project_kernel,
         "project",
-        (4, 128),
+        (2, 128),
         BF16,
         tp,
         shared(packed, "kv_1"),
         lam,
-        head_gain.reshape(1, 128),
+        head,
         out_weight,
-        tokens,
+        own,
         scalars=1,
         scratch=[pltpu.VMEM((64, 128), F32)],
     )
-    pieces = shared(block, KV_TP)
+    pieces = shared(block, KV_TP).reshape(256, 128)
     partial = call(
         mlp_kernel,
         "mlp",

time: 115 us -> 111 us (0.965)
  local copies, waits for them, and re-layouts: 3.25 us -> 0.23 us
  blocking collectives: 98.9 us -> 97 us
    unnamed x28 -> x14, local copies, waits for them, and re-layouts: 2.76 us -> 0.04 us
    all_to_all x5, blocking collectives: 82.4 us -> 80.3 us  [shared(): return lax.all_to_all(copies, axis, 0, 0, tiled=True)]
  transfers between devices with their start and end apart: 1 -> 1, of which waited for: 1 -> 0; matrix products, arithmetic and copies ran while one was open for 0% -> 0% of each run, Pallas kernels for 0% -> 1%
where the time goes in v3:
time: 111 us
  blocking collectives  97 us (87%)
  starting transfers between devices  8.73 us (8%)
  Pallas kernels  4.6 us (4%)
    all_to_all x5, blocking collectives, shared(): return lax.all_to_all(copies, axis, 0, 0, tiled=True)  80.3 us
    all_to_all x1, blocking collectives, shards(): sums = lax.all_to_all(partial.reshape(128, 1, 128), KV_TP, 0, 0, tiled=True)  16.7 us
    ppermute x1, starting transfers between devices, shards(): other = lax.ppermute(tokens, 'tp', [(0, 1), (1, 0)])  8.73 us
    pallas_call x6, Pallas kernels, call(): pl.pallas_call(kernel, name=name, out_shape=pltpu.VMEM(shape, dtype) if n...  3.59 us
  transfers between devices with their start and end apart: 1, of which 0 were waited for; matrix products, arithmetic and copies ran while one was open for 0% of the time, Pallas kernels for 1%

profile of v3, /device:TPU:1, one launch (start us, length us, event | category | flops | bytes accessed | tf_op | source)
XLA Modules:
  0.0 110.8 jit_solution(18382265313483694338)
XLA Ops:
  0.0 8.7 %collective-permute-start = (bf16[4,32]{1,0:T(4,128)(2,1)}, bf16[4,32]{1,0:T(4,128)(2,1)S(1)}, u32[]{:S(2)}, u32[]{:S(2)}) collective-permute-start(bf16[4,32]{1,0:T(4,128)(2,1)} %own_in.1), channel_id=1, source_target_pairs={{0,1},{1,0},{2,3},{3,2},{4,5},{5,4},{6,7},{7,6},{8,9},{9,8},{10,11... | collective-permute-start | bytes 776 | tf_op jit(solution)/shard_map/ppermute | solution.py:225
  8.8 1.0 prepare.1
  9.8 0.0 collective-permute-done.other_ref
  9.8 0.3 query.1
  10.1 16.8 %all_to_all.30 = f32[8,72,128]{2,1,0:T(8,128)S(1)} all-to-all(f32[8,72,128]{2,1,0:T(8,128)S(1)} %broadcast_in_dim.15), channel_id=1, replica_groups=mesh['dp'=4,'kv_0'=8,'kv_1'=8,'tp'=2] {'kv_0'}, dimensions={0} | all-to-all | bytes 589824 | tf_op jit(solution)/shard_map/all_to_all | solution.py:33
  26.9 0.0 copy-start.3
  26.9 0.0 copy-start.4
  27.0 17.2 %all_to_all.31.parts_ref = f32[8,72,128]{2,1,0:T(8,128)S(1)} all-to-all(f32[8,72,128]{2,1,0:T(8,128)S(1)} %broadcast_in_dim.16), channel_id=1, replica_groups=mesh['dp'=4,'kv_0'=8,'kv_1'=8,'tp'=2] {'kv_1'}, dimensions={0} | all-to-all | bytes 589824 | tf_op jit(solution)/shard_map/all_to_all | solution.py:33
  44.2 0.0 copy-done.3
  44.2 0.0 copy-done.4
  44.2 0.5 attend.1
  44.8 0.0 copy-start.2
  44.8 12.2 %all_to_all.32.parts_ref = bf16[8,144,128]{2,1,0:T(8,128)(2,1)S(1)} all-to-all(bf16[8,144,128]{2,1,0:T(8,128)(2,1)S(1)} %broadcast_in_dim.17), channel_id=1, replica_groups=mesh['dp'=4,'kv_0'=8,'kv_1'=8,'tp'=2] {'kv_0'}, dimensions={0} | all-to-all | bytes 589824 | tf_op jit(solution)/shard_map/all_to_all | solution.py:33
  57.0 0.0 copy-start.5
  57.0 0.4 merge.1
  57.4 0.0 copy-start.1
  57.4 0.0 copy-start
  57.4 13.6 %all_to_all.33.parts_ref = bf16[8,144,128]{2,1,0:T(8,128)(2,1)S(1)} all-to-all(bf16[8,144,128]{2,1,0:T(8,128)(2,1)S(1)} %broadcast_in_dim.18), channel_id=1, replica_groups=mesh['dp'=4,'kv_0'=8,'kv_1'=8,'tp'=2] {'kv_1'}, dimensions={0} | all-to-all | bytes 589824 | tf_op jit(solution)/shard_map/all_to_all | solution.py:33
  71.0 0.0 copy-done.5
  71.0 0.7 project.1
  71.8 0.0 copy-start.6
  71.8 20.6 %all_to_all.34 = bf16[128,2,128]{2,1,0:T(2,128)(2,1)S(1)} all-to-all(bf16[128,2,128]{2,1,0:T(2,128)(2,1)S(1)} %broadcast_in_dim.19), channel_id=1, replica_groups=mesh['dp'=4,'kv_0'=8,'kv_1'=8,'tp'=2] {'kv_0','kv_1','tp'}, dimensions={0} | all-to-all | bytes 131072 | tf_op jit(solution)/shard_map/all_to_all | solution.py:33
  92.4 0.0 copy-done.2
  92.4 0.0 copy-done.1
  92.4 0.0 copy-done
  92.4 0.0 copy-done.6
  92.4 1.0 mlp.1
  93.4 16.7 %all_to_all.35 = f32[128,1,128]{2,1,0:T(1,128)S(1)} all-to-all(f32[128,1,128]{2,1,0:T(1,128)S(1)} %bitcast.15), channel_id=1, replica_groups=mesh['dp'=4,'kv_0'=8,'kv_1'=8,'tp'=2] {'kv_0','kv_1','tp'}, dimensions={0} | all-to-all | bytes 131072 | tf_op jit(solution)/shard_map/all_to_all | solution.py:291
  110.1 0.7 total.1
  (6 shorter events, 0.2 us)
Async XLA Ops:
  0.0 9.8 %collective-permute-start = (bf16[4,32]{1,0:T(4,128)(2,1)}, bf16[4,32]{1,0:T(4,128)(2,1)S(1)}, u32[]{:S(2)}, u32[]{:S(2)}) collective-permute-start(bf16[4,32]{1,0:T(4,128)(2,1)} %own_in.1), channel_id=1, source_target_pairs={{0,1},{1,0},{2,3},{3,2},{4,5},{5,4},{6,7},{7,6},{8,9},{9,8},{10,11... | collective-permute-start | bytes 776 | tf_op jit(solution)/shard_map/ppermute | solution.py:225
  26.9 17.3 %copy-start.3 = (bf16[4,256,1,128]{3,1,2,0:T(8,128)(2,1)S(1)}, bf16[4,256,1,128]{3,1,2,0:T(8,128)(2,1)}, u32[]{:S(2)}) copy-start(bf16[4,256,1,128]{3,1,2,0:T(8,128)(2,1)} %param.16) | copy-start | bytes 786436
  26.9 17.2 %copy-start.4 = (bf16[4,256,1,128]{3,1,2,0:T(8,128)(2,1)S(1)}, bf16[4,256,1,128]{3,1,2,0:T(8,128)(2,1)}, u32[]{:S(2)}) copy-start(bf16[4,256,1,128]{3,1,2,0:T(8,128)(2,1)} %param.17) | copy-start | bytes 786436
  44.8 47.6 %copy-start.2 = (bf16[88,4096]{1,0:T(8,128)(2,1)S(1)}, bf16[88,4096]{1,0:T(8,128)(2,1)}, u32[]{:S(2)}) copy-start(bf16[88,4096]{1,0:T(8,128)(2,1)} %down_ref.1) | copy-start | bytes 2162692
  57.0 14.0 %copy-start.5 = (bf16[64,2048]{1,0:T(8,128)(2,1)S(1)}, bf16[64,2048]{1,0:T(8,128)(2,1)}, u32[]{:S(2)}) copy-start(bf16[64,2048]{1,0:T(8,128)(2,1)} %weight_ref.1) | copy-start | bytes 786436
  57.4 35.0 %copy-start.1 = (bf16[88,4096]{1,0:T(8,128)(2,1)S(1)}, bf16[88,4096]{1,0:T(8,128)(2,1)}, u32[]{:S(2)}) copy-start(bf16[88,4096]{1,0:T(8,128)(2,1)} %up_ref.1) | copy-start | bytes 2162692
  57.4 34.9 %copy-start = (bf16[88,4096]{1,0:T(8,128)(2,1)S(1)}, bf16[88,4096]{1,0:T(8,128)(2,1)}, u32[]{:S(2)}) copy-start(bf16[88,4096]{1,0:T(8,128)(2,1)} %gate_ref.1) | copy-start | bytes 2162692
  71.8 20.6 %copy-start.6 = (f32[4096]{0:T(1024)S(1)}, f32[4096]{0:T(1024)}, u32[]{:S(2)}) copy-start(f32[4096]{0:T(1024)} %param.21) | copy-start | bytes 49156

commit v4 on v3

--- a/solution.py
+++ b/solution.py
@@ -34,23 +34,26 @@
 
 
 def prepare_kernel(
-    kv_ref, own_in, weight_in, gain_in, lam_in, turn_in, head_in,
-    own_ref, weight_ref, gain_ref, lam_ref, turn_ref, head_ref, all_ref, row_ref, sems,
+    kv_ref, own_in, weight_in, gain_in, lam_in, turn_in, head_in, key_in, value_in,
+    own_ref, weight_ref, gain_ref, lam_ref, turn_ref, head_ref, cache_ref, all_ref, row_ref, sems,
 ):
+    away = pl.ds(2 - 2 * (kv_ref[0] // 8 % 2), 2)
     pairs = [
-        (weight_in, weight_ref), (own_in, own_ref), (gain_in, all_ref), (lam_in, row_ref),
-        (turn_in, turn_ref), (head_in, head_ref),
+        (weight_in, weight_ref), (key_in.at[away], cache_ref.at[0:2]),
+        (value_in.at[away], cache_ref.at[2:4]), (own_in, own_ref), (gain_in, all_ref),
+        (lam_in, row_ref), (turn_in, turn_ref), (head_in, head_ref),
     ]
     copies = [pltpu.make_async_copy(a, b, sems.at[k]) for k, (a, b) in enumerate(pairs)]
     for copy in copies:
         copy.start()
-    for copy in copies[1:]:
+    for copy in copies[3:]:
         copy.wait()
     line = all_ref[pl.ds(kv_ref[0] // 2, 1), :]
     gain_ref[...] = jnp.where(kv_ref[0] % 2 == 0, line, pltpu.roll(line, 64, 1))
-    picked = jnp.where(lanes((64, 16)) == rows((64, 16)) // 4, row_ref[...], 0.0)
-    lam_ref[...] = jnp.broadcast_to(jnp.sum(picked, axis=1, keepdims=True), (64, 128))
-    copies[0].wait()
+    picked = jnp.where(lanes((32, 16)) == rows((32, 16)) // 2, row_ref[...], 0.0)
+    lam_ref[...] = jnp.broadcast_to(jnp.sum(picked, axis=1, keepdims=True), (32, 128))
+    for copy in copies[:3]:
+        copy.wait()
 
 
 def query_kernel(tp_ref, own_ref, other_ref, gain_ref, weight_ref, out_ref):
@@ -61,11 +64,13 @@
     square = jnp.sum(x * x, axis=1, keepdims=True)
     scaled = (x * gain_ref[:, :64]).astype(BF16)
     q = jnp.dot(scaled, weight_ref[...], preferred_element_type=F32)
-    for h in range(16):
-        out_ref[4 * h : 4 * h + 4, :] = q[:, 128 * h : 128 * h + 128]
     wide = jnp.broadcast_to(square, (4, 128))
-    out_ref[64:68, :] = wide
-    out_ref[68:72, :] = wide
+    for pair in range(2):
+        two = slice(2 * pair, 2 * pair + 2)
+        for h in range(16):
+            out_ref[pair, 2 * h : 2 * h + 2, :] = q[two, 128 * h : 128 * h + 128]
+        for k in range(4):
+            out_ref[pair, 32 + 2 * k : 34 + 2 * k, :] = wide[two]
 
 
 def pack(values, lse):
@@ -77,66 +82,93 @@
     return values.astype(BF16), tail.astype(BF16)
 
 
-def attend_kernel(parts_ref, turn_ref, key_ref, value_ref, out_ref):
-    total = parts_ref[0]
-    for k in range(1, 8):
-        total = total + parts_ref[k]
-    scale = lax.rsqrt(total[64:72] * (1.0 / 4096) + EPS)
-    q = (total[:64].reshape(8, 8, 128) * scale[None]).reshape(64, 128)
-    lane = lanes((64, 128))
+def attend_kernel(pair_ref, part_ref, turn_ref, key_ref, value_ref, cache_ref, out_ref):
+    total = part_ref[...]
+    scale = lax.rsqrt(total[32:40] * (1.0 / 4096) + EPS)
+    q = (total[:32].reshape(4, 8, 128) * scale[None]).reshape(32, 128)
+    lane = lanes((32, 128))
     swapped = jnp.where(lane % 64 < 32, pltpu.roll(q, 96, 1), pltpu.roll(q, 32, 1))
     turned = q * turn_ref[0:1] + swapped * turn_ref[1:2]
     both = jnp.concatenate(
         [jnp.where(lane < 64, turned, 0.0), jnp.where(lane < 64, 0.0, turned)], axis=0
     ).astype(BF16)
-    row = rows((128, 256)) % 4
-    scores = inner_last(both, key_ref[0])
-    for b in range(1, 4):
-        scores = jnp.where(row == b, inner_last(both, key_ref[b]), scores)
-    scores = scores * 0.125
+    here = 2 * pair_ref[0]
+
+    def against(b):
+        near = inner_last(both, key_ref[here + b])
+        return jnp.concatenate([near, inner_last(both, cache_ref[b])], axis=1)
+
+    scores = jnp.where(rows((64, 512)) % 2 == 0, against(0), against(1)) * 0.125
     peak = jnp.max(scores, axis=1, keepdims=True)
     e = jnp.exp(scores - peak)
     total_e = jnp.sum(e, axis=1, keepdims=True)
     probs = e.astype(BF16)
-    row_v = rows((128, 128)) % 4
-    value = jnp.dot(probs, value_ref[0], preferred_element_type=F32)
-    for b in range(1, 4):
-        value = jnp.where(
-            row_v == b, jnp.dot(probs, value_ref[b], preferred_element_type=F32), value
-        )
-    value = value / total_e
+
+    def valued(b):
+        near = jnp.dot(probs[:, :256], value_ref[here + b], preferred_element_type=F32)
+        return near + jnp.dot(probs[:, 256:], cache_ref[2 + b], preferred_element_type=F32)
+
+    value = jnp.where(rows((64, 128)) % 2 == 0, valued(0), valued(1)) / total_e
     lse = peak + jnp.log(total_e)
-    eye = rows((128, 128)) == lanes((128, 128))
+    eye = rows((64, 128)) == lanes((64, 128))
     lse_row = jnp.sum(jnp.where(eye, lse, 0.0), axis=0, keepdims=True)
-    out_ref[:128, :], out_ref[128:, :] = pack(value, lse_row)
-
-
-def merged(parts_ref):
+    out_ref[:64, :], out_ref[64:, :] = pack(value, lse_row)
+
+
+def lse_of(parts_ref):
     tails = []
     for k in range(8):
-        tail = parts_ref[k, 128:, :].astype(F32)
+        tail = parts_ref[k, 64:, :].astype(F32)
         tails.append(tail[0:1] + tail[1:2] + tail[2:3])
-    lse = jnp.concatenate(tails, axis=0)
+    return jnp.concatenate(tails, axis=0)
+
+
+def weighed(parts_ref, share, slots):
+    value = 0.0
+    for k in slots:
+        value = value + share[:64, k : k + 1] * parts_ref[k, :64, :].astype(F32)
+    return value
+
+
+def merge_kernel(parts_ref, out_ref):
+    lse = lse_of(parts_ref)
     peak = jnp.max(lse, axis=0, keepdims=True)
     e = jnp.exp(lse - peak)
     total = jnp.sum(e, axis=0, keepdims=True)
+    value = weighed(parts_ref, (e / total).T, range(8))
+    out_ref[:64, :], out_ref[64:, :] = pack(value, peak + jnp.log(total))
+
+
+def project_kernel(tp_ref, parts_ref, lam_ref, gain_ref, weight_ref, own_ref, out_ref, heads_ref):
+    lse = lse_of(parts_ref)
+    even = rows((8, 128)) % 2 == 0
+    low = jnp.finfo(F32).min
+    peak = jnp.where(
+        even,
+        jnp.max(jnp.where(even, lse, low), axis=0, keepdims=True),
+        jnp.max(jnp.where(even, low, lse), axis=0, keepdims=True),
+    )
+    e = jnp.exp(lse - peak)
+    total = jnp.where(
+        even,
+        jnp.sum(jnp.where(even, e, 0.0), axis=0, keepdims=True),
+        jnp.sum(jnp.where(even, 0.0, e), axis=0, keepdims=True),
+    )
     share = (e / total).T
-    value = share[:, 0:1] * parts_ref[0, :128, :].astype(F32)
-    for k in range(1, 8):
-        value = value + share[:, k : k + 1] * parts_ref[k, :128, :].astype(F32)
-    return value, peak + jnp.log(total)
-
-
-def merge_kernel(parts_ref, out_ref):
-    out_ref[:128, :], out_ref[128:, :] = pack(*merged(parts_ref))
-
-
-def project_kernel(tp_ref, parts_ref, lam_ref, gain_ref, weight_ref, own_ref, out_ref, heads_ref):
-    value, _ = merged(parts_ref)
-    difference = value[:64] - lam_ref[...] * value[64:]
-    norm = lax.rsqrt(jnp.mean(difference * difference, axis=1, keepdims=True) + EPS)
-    heads_ref[...] = difference * norm * gain_ref[...]
-    head_out = jnp.concatenate([heads_ref[4 * h : 4 * h + 4, :] for h in range(16)], axis=1)
+    for pair in range(2):
+        value = weighed(parts_ref, share, range(pair, 8, 2))
+        difference = value[:32] - lam_ref[...] * value[32:]
+        norm = lax.rsqrt(jnp.mean(difference * difference, axis=1, keepdims=True) + EPS)
+        heads_ref[32 * pair : 32 * pair + 32, :] = difference * norm * gain_ref[...]
+    head_out = jnp.concatenate(
+        [
+            jnp.concatenate(
+                [heads_ref[32 * pair + 2 * h : 32 * pair + 2 * h + 2, :] for h in range(16)], axis=1
+            )
+            for pair in range(2)
+        ],
+        axis=0,
+    )
     part = inner_last(head_out.astype(BF16), weight_ref[...])
     part = part.astype(BF16).astype(F32)
     lane = lanes((4, 64))
@@ -189,7 +221,6 @@
     near = [pltpu.with_memory_space_constraint(x, pltpu.VMEM) for x in args[scalars:]]
     return pl.pallas_call(
         kernel,
-        name=name,
         out_shape=pltpu.VMEM(shape, dtype) if name != "total" else SHAPE(shape, dtype),
         in_specs=[smem] * scalars + [vmem] * len(near),
         out_specs=vmem,
@@ -224,23 +255,27 @@
     at = lax.axis_index(KV_TP).astype(jnp.int32).reshape(1)
     other = lax.ppermute(tokens, "tp", [(0, 1), (1, 0)])
     turn = turn_tables(key_cache.shape[1] * lax.axis_size(KV))
-    own, weight, gain, lam, turn, head = pl.pallas_call(
+    keys = key_cache.reshape(4, 256, 128)
+    values = value_cache.reshape(4, 256, 128)
+    pair = (kv // 8 % 2).astype(jnp.int32).reshape(1)
+    own, weight, gain, lam, turn, head, cache = pl.pallas_call(
         prepare_kernel,
         name="prepare",
         out_shape=[
             pltpu.VMEM((4, 32), BF16),
             pltpu.VMEM((64, 2048), BF16),
             pltpu.VMEM((1, 128), F32),
-            pltpu.VMEM((64, 128), F32),
+            pltpu.VMEM((32, 128), F32),
             pltpu.VMEM((8, 128), F32),
             pltpu.VMEM((1, 128), F32),
+            pltpu.VMEM((4, 256, 128), BF16),
         ],
-        in_specs=[pl.BlockSpec(memory_space=pltpu.SMEM)] + [pl.BlockSpec(memory_space=pl.ANY)] * 6,
-        out_specs=[pl.BlockSpec(memory_space=pltpu.VMEM)] * 6,
+        in_specs=[pl.BlockSpec(memory_space=pltpu.SMEM)] + [pl.BlockSpec(memory_space=pl.ANY)] * 8,
+        out_specs=[pl.BlockSpec(memory_space=pltpu.VMEM)] * 7,
         scratch_shapes=[
             pltpu.VMEM((32, 128), F32),
             pltpu.VMEM((1, 16), F32),
-            pltpu.SemaphoreType.DMA((6,)),
+            pltpu.SemaphoreType.DMA((8,)),
         ],
     )(
         kv.astype(jnp.int32).reshape(1),
@@ -250,22 +285,38 @@
         head_lambda.reshape(1, 16),
         turn,
         head_gain.reshape(1, 128),
-    )
-    part = call(query_kernel, "query", (72, 128), F32, tp, own, other, gain, weight, scalars=1)
-    part, at = lax.optimization_barrier((part, at))
-    part = jnp.sum(shared(part, "kv_0"), axis=0)
+        keys,
+        values,
+    )
+    part = call(query_kernel, "query", (2, 40, 128), F32, tp, own, other, gain, weight, scalars=1)
+    part, at, pair = lax.optimization_barrier((part, at, pair))
+    copies = jnp.broadcast_to(part[None], (4, 2, 40, 128)).reshape(8, 40, 128)
+    part = jnp.sum(lax.all_to_all(copies, "kv_0", 0, 0, tiled=True), axis=0)
+    part, cache = lax.optimization_barrier((part, cache))
+    cache = lax.ppermute(cache, "kv_0", [(z, z ^ 1) for z in range(8)])
     parts = shared(part, "kv_1")
-    keys = key_cache.reshape(4, 256, 128)
-    values = value_cache.reshape(4, 256, 128)
-    packed = call(attend_kernel, "attend", (144, 128), BF16, parts, turn, keys, values)
-    packed = call(merge_kernel, "merge", (144, 128), BF16, shared(packed, "kv_0"))
+    part = jnp.sum(parts, axis=0)
+    packed = call(
+        attend_kernel,
+        "attend",
+        (80, 128),
+        BF16,
+        pair,
+        part,
+        turn,
+        keys,
+        values,
+        cache,
+        scalars=1,
+    )
+    packed = call(merge_kernel, "merge", (80, 128), BF16, shared(packed, "kv_1"))
     block = call(
         project_kernel,
         "project",
         (2, 128),
         BF16,
         tp,
-        shared(packed, "kv_1"),
+        shared(packed, "kv_0"),
         lam,
         head,
         out_weight,

time: 111 us -> 107 us (0.964)
  blocking collectives: 97 us -> 76.6 us
  starting transfers between devices: 8.73 us -> 17.6 us
  waiting for transfers between devices: 0.01 us -> 6.42 us
    all_to_all x5 -> x3, blocking collectives: 80.3 us -> 46.5 us  [shared(): return lax.all_to_all(copies, axis, 0, 0, tiled=True)]
    all_to_all x0 -> x1, blocking collectives: none -> 13.5 us  [shards(): part = jnp.sum(lax.all_to_all(copies, 'kv_0', 0, 0, tiled=True), axis=0)]
    all_to_all x0 -> x1, starting transfers between devices: none -> 6.95 us  [shared(): return lax.all_to_all(copies, axis, 0, 0, tiled=True)]
    all_to_all x0 -> x1, waiting for transfers between devices: none -> 6.41 us  [shared(): return lax.all_to_all(copies, axis, 0, 0, tiled=True)]
    ppermute x0 -> x1, starting transfers between devices: none -> 1.91 us  [shards(): cache = lax.ppermute(cache, 'kv_0', [(z, z ^ 1) for z in range(8)])]
  transfers between devices with their start and end apart: 1 -> 3, of which waited for: 0 -> 1; matrix products, arithmetic and copies ran while one was open for 0% -> 0% of each run, Pallas kernels for 1% -> 1%
where the time goes in v4:
time: 107 us; the launch traced here: 106 us
  blocking collectives  76.6 us (72%)
  starting transfers between devices  17.6 us (16%)
  waiting for transfers between devices  6.42 us (6%)
  Pallas kernels  4.47 us (4%)
    all_to_all x3, blocking collectives, shared(): return lax.all_to_all(copies, axis, 0, 0, tiled=True)  46.5 us
    all_to_all x1, blocking collectives, shards(): sums = lax.all_to_all(partial.reshape(128, 1, 128), KV_TP, 0, 0, tiled=True)  16.7 us
    all_to_all x1, blocking collectives, shards(): part = jnp.sum(lax.all_to_all(copies, 'kv_0', 0, 0, tiled=True), axis=0)  13.5 us
    ppermute x1, starting transfers between devices, shards(): other = lax.ppermute(tokens, 'tp', [(0, 1), (1, 0)])  8.73 us
    all_to_all x1, starting transfers between devices, shared(): return lax.all_to_all(copies, axis, 0, 0, tiled=True)  6.95 us
    all_to_all x1, waiting for transfers between devices, shared(): return lax.all_to_all(copies, axis, 0, 0, tiled=True)  6.41 us
    pallas_call x6, Pallas kernels, call(): pl.pallas_call(kernel, out_shape=pltpu.VMEM(shape, dtype) if name != 'tot...  3.35 us
  transfers between devices with their start and end apart: 3, of which 1 were waited for; matrix products, arithmetic and copies ran while one was open for 0% of the time, Pallas kernels for 1%

profile of v4, /device:TPU:1, one launch (start us, length us, event | category | flops | bytes accessed | tf_op | source)
XLA Modules:
  0.0 106.2 jit_solution(8344513441699603249)
XLA Ops:
  0.0 8.7 %collective-permute-start = (bf16[4,32]{1,0:T(4,128)(2,1)}, bf16[4,32]{1,0:T(4,128)(2,1)S(1)}, u32[]{:S(2)}, u32[]{:S(2)}) collective-permute-start(bf16[4,32]{1,0:T(4,128)(2,1)} %own_in.1), channel_id=1, source_target_pairs={{0,1},{1,0},{2,3},{3,2},{4,5},{5,4},{6,7},{7,6},{8,9},{9,8},{10,11... | collective-permute-start | bytes 776 | tf_op jit(solution)/shard_map/ppermute | solution.py:256
  8.8 1.1 %prepare.1 = (bf16[4,32]{1,0:T(4,128)(2,1)S(1)}, bf16[64,2048]{1,0:T(8,128)(2,1)S(1)}, f32[1,128]{1,0:T(1,128)S(1)}, f32[32,128]{1,0:T(8,128)S(1)}, f32[8,128]{1...) custom-call(s32[1]{0:T(128)} %bitcast.1.kv_ref, bf16[4,32]{1,0:T(4,128)(2,1)} %own_in.1, ...), custom_call_target="tpu_custom_call" | custom-call | tf_op jit(solution)/shard_map/prepare/pallas_call | solution.py:261
  9.9 0.0 collective-permute-done.other_ref
  9.9 0.3 shard_map.127
  10.2 13.5 %all_to_all.30 = f32[8,40,128]{2,1,0:T(8,128)S(1)} all-to-all(f32[8,40,128]{2,1,0:T(8,128)S(1)} %bitcast.24), channel_id=1, replica_groups=mesh['dp'=4,'kv_0'=8,'kv_1'=8,'tp'=2] {'kv_0'}, dimensions={0} | all-to-all | bytes 327680 | tf_op jit(solution)/shard_map/all_to_all | solution.py:294
  23.7 0.0 copy-start.1
  23.7 0.7 broadcast_in_dim.19
  24.4 7.0 %all-to-all-start.1 = ((f32[8,40,128]{2,1,0:T(8,128)}), f32[8,40,128]{2,1,0:T(8,128)S(1)}, u32[]{:S(2)}, u32[]{:S(2)}) async-start(f32[8,40,128]{2,1,0:T(8,128)} %broadcast_in_dim.19), calls=%async_computation.1 | async-start | bytes 327680 | tf_op jit(solution)/shard_map/all_to_all | solution.py:33
  31.4 1.9 %collective-permute-start.1 = (bf16[4,256,128]{2,1,0:T(8,128)(2,1)S(1)}, bf16[4,256,128]{2,1,0:T(8,128)(2,1)S(1)}, u32[]{:S(2)}, u32[]{:S(2)}) collective-permute-start(bf16[4,256,128]{2,1,0:T(8,128)(2,1)S(1)} %get-tuple-element.26), channel_id=1, source_target_pairs={{0,16},{16,0},{32,48},{48,32},{64,80},{80,64},{96,112},{112,96},{1... | collective-permute-start | bytes 786440 | tf_op jit(solution)/shard_map/ppermute | solution.py:296
  33.3 6.4 %all-to-all-done.1 = f32[8,40,128]{2,1,0:T(8,128)S(1)} async-done(((f32[8,40,128]{2,1,0:T(8,128)}), f32[8,40,128]{2,1,0:T(8,128)S(1)}, u32[]{:S(2)}, u32[]{:S(2)}) %all-to-all-start.1) | async-done | bytes 163872 | tf_op jit(solution)/shard_map/all_to_all | solution.py:33
  39.7 0.0 collective-permute-done.1.cache_ref
  39.7 0.0 copy-done.1
  39.7 0.0 copy-done
  39.7 0.0 copy-start.4
  39.8 0.5 shard_map.128
  40.3 0.0 copy-start.5
  40.3 0.0 copy-start.3
  40.3 14.0 %all_to_all.31.parts_ref = bf16[8,80,128]{2,1,0:T(8,128)(2,1)S(1)} all-to-all(bf16[8,80,128]{2,1,0:T(8,128)(2,1)S(1)} %broadcast_in_dim.20), channel_id=1, replica_groups=mesh['dp'=4,'kv_0'=8,'kv_1'=8,'tp'=2] {'kv_1'}, dimensions={0} | all-to-all | bytes 327680 | tf_op jit(solution)/shard_map/all_to_all | solution.py:33
  54.3 0.3 shard_map.129
  54.6 11.2 %all_to_all.32.parts_ref = bf16[8,80,128]{2,1,0:T(8,128)(2,1)S(1)} all-to-all(bf16[8,80,128]{2,1,0:T(8,128)(2,1)S(1)} %broadcast_in_dim.21), channel_id=1, replica_groups=mesh['dp'=4,'kv_0'=8,'kv_1'=8,'tp'=2] {'kv_0'}, dimensions={0} | all-to-all | bytes 327680 | tf_op jit(solution)/shard_map/all_to_all | solution.py:33
  65.8 0.0 copy-done.5
  65.8 0.6 shard_map.130
  66.4 0.1 broadcast_in_dim.22
  66.5 0.0 copy-start.6
  66.5 21.3 %all_to_all.33 = bf16[128,2,128]{2,1,0:T(2,128)(2,1)S(1)} all-to-all(bf16[128,2,128]{2,1,0:T(2,128)(2,1)S(1)} %broadcast_in_dim.22), channel_id=1, replica_groups=mesh['dp'=4,'kv_0'=8,'kv_1'=8,'tp'=2] {'kv_0','kv_1','tp'}, dimensions={0} | all-to-all | bytes 131072 | tf_op jit(solution)/shard_map/all_to_all | solution.py:33
  87.8 0.0 copy-done.4
  87.8 0.0 copy-done.3
  87.8 0.0 copy-done.2
  87.8 0.0 copy-done.6
  87.8 1.0 shard_map.131
  88.8 16.7 %all_to_all.34 = f32[128,1,128]{2,1,0:T(1,128)S(1)} all-to-all(f32[128,1,128]{2,1,0:T(1,128)S(1)} %bitcast.21), channel_id=1, replica_groups=mesh['dp'=4,'kv_0'=8,'kv_1'=8,'tp'=2] {'kv_0','kv_1','tp'}, dimensions={0} | all-to-all | bytes 131072 | tf_op jit(solution)/shard_map/all_to_all | solution.py:342
  105.5 0.7 shard_map.132
  (7 shorter events, 0.1 us)
Async XLA Ops:
  0.0 9.9 %collective-permute-start = (bf16[4,32]{1,0:T(4,128)(2,1)}, bf16[4,32]{1,0:T(4,128)(2,1)S(1)}, u32[]{:S(2)}, u32[]{:S(2)}) collective-permute-start(bf16[4,32]{1,0:T(4,128)(2,1)} %own_in.1), channel_id=1, source_target_pairs={{0,1},{1,0},{2,3},{3,2},{4,5},{5,4},{6,7},{7,6},{8,9},{9,8},{10,11... | collective-permute-start | bytes 776 | tf_op jit(solution)/shard_map/ppermute | solution.py:256
  23.7 16.0 %copy-start.1 = (bf16[4,256,1,128]{3,1,2,0:T(8,128)(2,1)S(1)}, bf16[4,256,1,128]{3,1,2,0:T(8,128)(2,1)}, u32[]{:S(2)}) copy-start(bf16[4,256,1,128]{3,1,2,0:T(8,128)(2,1)} %param.17) | copy-start | bytes 786436
  24.4 15.3 %copy-start = (bf16[4,256,1,128]{3,1,2,0:T(8,128)(2,1)S(1)}, bf16[4,256,1,128]{3,1,2,0:T(8,128)(2,1)}, u32[]{:S(2)}) copy-start(bf16[4,256,1,128]{3,1,2,0:T(8,128)(2,1)} %param.16) | copy-start | bytes 786436
  24.4 15.3 %all-to-all-start.1 = ((f32[8,40,128]{2,1,0:T(8,128)}), f32[8,40,128]{2,1,0:T(8,128)S(1)}, u32[]{:S(2)}, u32[]{:S(2)}) async-start(f32[8,40,128]{2,1,0:T(8,128)} %broadcast_in_dim.19), calls=%async_computation.1 | async-start | bytes 327680 | tf_op jit(solution)/shard_map/all_to_all | solution.py:33
  31.4 8.4 %collective-permute-start.1 = (bf16[4,256,128]{2,1,0:T(8,128)(2,1)S(1)}, bf16[4,256,128]{2,1,0:T(8,128)(2,1)S(1)}, u32[]{:S(2)}, u32[]{:S(2)}) collective-permute-start(bf16[4,256,128]{2,1,0:T(8,128)(2,1)S(1)} %get-tuple-element.26), channel_id=1, source_target_pairs={{0,16},{16,0},{32,48},{48,32},{64,80},{80,64},{96,112},{112,96},{1... | collective-permute-start | bytes 786440 | tf_op jit(solution)/shard_map/ppermute | solution.py:296
  39.7 48.0 %copy-start.4 = (bf16[88,4096]{1,0:T(8,128)(2,1)S(1)}, bf16[88,4096]{1,0:T(8,128)(2,1)}, u32[]{:S(2)}) copy-start(bf16[88,4096]{1,0:T(8,128)(2,1)} %down_ref.1) | copy-start | bytes 2162692
  40.3 25.6 %copy-start.5 = (bf16[64,2048]{1,0:T(8,128)(2,1)S(1)}, bf16[64,2048]{1,0:T(8,128)(2,1)}, u32[]{:S(2)}) copy-start(bf16[64,2048]{1,0:T(8,128)(2,1)} %weight_ref.1) | copy-start | bytes 786436
  40.3 47.5 %copy-start.3 = (bf16[88,4096]{1,0:T(8,128)(2,1)S(1)}, bf16[88,4096]{1,0:T(8,128)(2,1)}, u32[]{:S(2)}) copy-start(bf16[88,4096]{1,0:T(8,128)(2,1)} %up_ref.1) | copy-start | bytes 2162692
  54.3 33.5 %copy-start.2 = (bf16[88,4096]{1,0:T(8,128)(2,1)S(1)}, bf16[88,4096]{1,0:T(8,128)(2,1)}, u32[]{:S(2)}) copy-start(bf16[88,4096]{1,0:T(8,128)(2,1)} %gate_ref.1) | copy-start | bytes 2162692
  66.5 21.3 %copy-start.6 = (f32[4096]{0:T(1024)S(1)}, f32[4096]{0:T(1024)}, u32[]{:S(2)}) copy-start(f32[4096]{0:T(1024)} %param.21) | copy-start | bytes 49156

commit v5 on v4

--- a/solution.py
+++ b/solution.py
@@ -77,7 +77,7 @@
     high = lse.astype(BF16).astype(F32)
     mid = (lse - high).astype(BF16).astype(F32)
     low = lse - high - mid
-    at = rows((16, 128))
+    at = rows((8, 128))
     tail = jnp.where(at == 0, high, jnp.where(at == 1, mid, jnp.where(at == 2, low, 0.0)))
     return values.astype(BF16), tail.astype(BF16)
 
@@ -299,7 +299,7 @@
     packed = call(
         attend_kernel,
         "attend",
-        (80, 128),
+        (72, 128),
         BF16,
         pair,
         part,
@@ -309,7 +309,7 @@
         cache,
         scalars=1,
     )
-    packed = call(merge_kernel, "merge", (80, 128), BF16, shared(packed, "kv_1"))
+    packed = call(merge_kernel, "merge", (72, 128), BF16, shared(packed, "kv_1"))
     block = call(
         project_kernel,
         "project",

time: 107 us -> 106 us (level)
  no operation moved by 1% of the time
where the time goes in v5:
time: 106 us
  blocking collectives  76.3 us (72%)
  starting transfers between devices  17.6 us (17%)
  waiting for transfers between devices  6.42 us (6%)
  Pallas kernels  4.47 us (4%)
    all_to_all x3, blocking collectives, shared(): return lax.all_to_all(copies, axis, 0, 0, tiled=True)  46.1 us
    all_to_all x1, blocking collectives, shards(): sums = lax.all_to_all(partial.reshape(128, 1, 128), KV_TP, 0, 0, tiled=True)  16.7 us
    all_to_all x1, blocking collectives, shards(): part = jnp.sum(lax.all_to_all(copies, 'kv_0', 0, 0, tiled=True), axis=0)  13.5 us
    ppermute x1, starting transfers between devices, shards(): other = lax.ppermute(tokens, 'tp', [(0, 1), (1, 0)])  8.73 us
    all_to_all x1, starting transfers between devices, shared(): return lax.all_to_all(copies, axis, 0, 0, tiled=True)  6.95 us
    all_to_all x1, waiting for transfers between devices, shared(): return lax.all_to_all(copies, axis, 0, 0, tiled=True)  6.41 us
    pallas_call x6, Pallas kernels, call(): pl.pallas_call(kernel, out_shape=pltpu.VMEM(shape, dtype) if name != 'tot...  3.35 us
  transfers between devices with their start and end apart: 3, of which 1 were waited for; matrix products, arithmetic and copies ran while one was open for 0% of the time, Pallas kernels for 1%

profile of v5, /device:TPU:1, one launch (start us, length us, event | category | flops | bytes accessed | tf_op | source)
XLA Modules:
  0.0 105.8 jit_solution(2185080037705887029)
XLA Ops:
  0.0 8.7 %collective-permute-start = (bf16[4,32]{1,0:T(4,128)(2,1)}, bf16[4,32]{1,0:T(4,128)(2,1)S(1)}, u32[]{:S(2)}, u32[]{:S(2)}) collective-permute-start(bf16[4,32]{1,0:T(4,128)(2,1)} %own_in.1), channel_id=1, source_target_pairs={{0,1},{1,0},{2,3},{3,2},{4,5},{5,4},{6,7},{7,6},{8,9},{9,8},{10,11... | collective-permute-start | bytes 776 | tf_op jit(solution)/shard_map/ppermute | solution.py:256
  8.8 1.1 %prepare.1 = (bf16[4,32]{1,0:T(4,128)(2,1)S(1)}, bf16[64,2048]{1,0:T(8,128)(2,1)S(1)}, f32[1,128]{1,0:T(1,128)S(1)}, f32[32,128]{1,0:T(8,128)S(1)}, f32[8,128]{1...) custom-call(s32[1]{0:T(128)} %bitcast.1.kv_ref, bf16[4,32]{1,0:T(4,128)(2,1)} %own_in.1, ...), custom_call_target="tpu_custom_call" | custom-call | tf_op jit(solution)/shard_map/prepare/pallas_call | solution.py:261
  9.9 0.0 collective-permute-done.other_ref
  9.9 0.3 shard_map.127
  10.2 13.5 %all_to_all.30 = f32[8,40,128]{2,1,0:T(8,128)S(1)} all-to-all(f32[8,40,128]{2,1,0:T(8,128)S(1)} %bitcast.24), channel_id=1, replica_groups=mesh['dp'=4,'kv_0'=8,'kv_1'=8,'tp'=2] {'kv_0'}, dimensions={0} | all-to-all | bytes 327680 | tf_op jit(solution)/shard_map/all_to_all | solution.py:294
  23.7 0.0 copy-start.1
  23.7 0.7 broadcast_in_dim.19
  24.4 7.0 %all-to-all-start.1 = ((f32[8,40,128]{2,1,0:T(8,128)}), f32[8,40,128]{2,1,0:T(8,128)S(1)}, u32[]{:S(2)}, u32[]{:S(2)}) async-start(f32[8,40,128]{2,1,0:T(8,128)} %broadcast_in_dim.19), calls=%async_computation.1 | async-start | bytes 327680 | tf_op jit(solution)/shard_map/all_to_all | solution.py:33
  31.4 1.9 %collective-permute-start.1 = (bf16[4,256,128]{2,1,0:T(8,128)(2,1)S(1)}, bf16[4,256,128]{2,1,0:T(8,128)(2,1)S(1)}, u32[]{:S(2)}, u32[]{:S(2)}) collective-permute-start(bf16[4,256,128]{2,1,0:T(8,128)(2,1)S(1)} %get-tuple-element.26), channel_id=1, source_target_pairs={{0,16},{16,0},{32,48},{48,32},{64,80},{80,64},{96,112},{112,96},{1... | collective-permute-start | bytes 786440 | tf_op jit(solution)/shard_map/ppermute | solution.py:296
  33.3 6.4 %all-to-all-done.1 = f32[8,40,128]{2,1,0:T(8,128)S(1)} async-done(((f32[8,40,128]{2,1,0:T(8,128)}), f32[8,40,128]{2,1,0:T(8,128)S(1)}, u32[]{:S(2)}, u32[]{:S(2)}) %all-to-all-start.1) | async-done | bytes 163872 | tf_op jit(solution)/shard_map/all_to_all | solution.py:33
  39.7 0.0 collective-permute-done.1.cache_ref
  39.7 0.0 copy-done.1
  39.7 0.0 copy-done
  39.7 0.0 copy-start.4
  39.8 0.5 shard_map.128
  40.3 0.0 copy-start.5
  40.3 0.0 copy-start.2
  40.3 0.0 copy-start.3
  40.3 13.8 %all_to_all.31.parts_ref = bf16[8,72,128]{2,1,0:T(8,128)(2,1)S(1)} all-to-all(bf16[8,72,128]{2,1,0:T(8,128)(2,1)S(1)} %broadcast_in_dim.20), channel_id=1, replica_groups=mesh['dp'=4,'kv_0'=8,'kv_1'=8,'tp'=2] {'kv_1'}, dimensions={0} | all-to-all | bytes 294912 | tf_op jit(solution)/shard_map/all_to_all | solution.py:33
  54.2 0.3 shard_map.129
  54.5 11.0 %all_to_all.32.parts_ref = bf16[8,72,128]{2,1,0:T(8,128)(2,1)S(1)} all-to-all(bf16[8,72,128]{2,1,0:T(8,128)(2,1)S(1)} %broadcast_in_dim.21), channel_id=1, replica_groups=mesh['dp'=4,'kv_0'=8,'kv_1'=8,'tp'=2] {'kv_0'}, dimensions={0} | all-to-all | bytes 294912 | tf_op jit(solution)/shard_map/all_to_all | solution.py:33
  65.5 0.0 copy-done.5
  65.5 0.6 shard_map.130
  66.1 0.1 broadcast_in_dim.22
  66.1 0.0 copy-start.6
  66.2 21.3 %all_to_all.33 = bf16[128,2,128]{2,1,0:T(2,128)(2,1)S(1)} all-to-all(bf16[128,2,128]{2,1,0:T(2,128)(2,1)S(1)} %broadcast_in_dim.22), channel_id=1, replica_groups=mesh['dp'=4,'kv_0'=8,'kv_1'=8,'tp'=2] {'kv_0','kv_1','tp'}, dimensions={0} | all-to-all | bytes 131072 | tf_op jit(solution)/shard_map/all_to_all | solution.py:33
  87.4 0.0 copy-done.4
  87.4 0.0 copy-done.3
  87.4 0.0 copy-done.6
  87.5 1.0 shard_map.131
  88.5 16.7 %all_to_all.34 = f32[128,1,128]{2,1,0:T(1,128)S(1)} all-to-all(f32[128,1,128]{2,1,0:T(1,128)S(1)} %bitcast.21), channel_id=1, replica_groups=mesh['dp'=4,'kv_0'=8,'kv_1'=8,'tp'=2] {'kv_0','kv_1','tp'}, dimensions={0} | all-to-all | bytes 131072 | tf_op jit(solution)/shard_map/all_to_all | solution.py:342
  105.2 0.7 shard_map.132
  (7 shorter events, 0.1 us)
Async XLA Ops:
  0.0 9.9 %collective-permute-start = (bf16[4,32]{1,0:T(4,128)(2,1)}, bf16[4,32]{1,0:T(4,128)(2,1)S(1)}, u32[]{:S(2)}, u32[]{:S(2)}) collective-permute-start(bf16[4,32]{1,0:T(4,128)(2,1)} %own_in.1), channel_id=1, source_target_pairs={{0,1},{1,0},{2,3},{3,2},{4,5},{5,4},{6,7},{7,6},{8,9},{9,8},{10,11... | collective-permute-start | bytes 776 | tf_op jit(solution)/shard_map/ppermute | solution.py:256
  23.7 16.0 %copy-start.1 = (bf16[4,256,1,128]{3,1,2,0:T(8,128)(2,1)S(1)}, bf16[4,256,1,128]{3,1,2,0:T(8,128)(2,1)}, u32[]{:S(2)}) copy-start(bf16[4,256,1,128]{3,1,2,0:T(8,128)(2,1)} %param.17) | copy-start | bytes 786436
  24.4 15.3 %copy-start = (bf16[4,256,1,128]{3,1,2,0:T(8,128)(2,1)S(1)}, bf16[4,256,1,128]{3,1,2,0:T(8,128)(2,1)}, u32[]{:S(2)}) copy-start(bf16[4,256,1,128]{3,1,2,0:T(8,128)(2,1)} %param.16) | copy-start | bytes 786436
  24.4 15.3 %all-to-all-start.1 = ((f32[8,40,128]{2,1,0:T(8,128)}), f32[8,40,128]{2,1,0:T(8,128)S(1)}, u32[]{:S(2)}, u32[]{:S(2)}) async-start(f32[8,40,128]{2,1,0:T(8,128)} %broadcast_in_dim.19), calls=%async_computation.1 | async-start | bytes 327680 | tf_op jit(solution)/shard_map/all_to_all | solution.py:33
  31.4 8.4 %collective-permute-start.1 = (bf16[4,256,128]{2,1,0:T(8,128)(2,1)S(1)}, bf16[4,256,128]{2,1,0:T(8,128)(2,1)S(1)}, u32[]{:S(2)}, u32[]{:S(2)}) collective-permute-start(bf16[4,256,128]{2,1,0:T(8,128)(2,1)S(1)} %get-tuple-element.26), channel_id=1, source_target_pairs={{0,16},{16,0},{32,48},{48,32},{64,80},{80,64},{96,112},{112,96},{1... | collective-permute-start | bytes 786440 | tf_op jit(solution)/shard_map/ppermute | solution.py:296
  39.7 47.7 %copy-start.4 = (bf16[88,4096]{1,0:T(8,128)(2,1)S(1)}, bf16[88,4096]{1,0:T(8,128)(2,1)}, u32[]{:S(2)}) copy-start(bf16[88,4096]{1,0:T(8,128)(2,1)} %down_ref.1) | copy-start | bytes 2162692
  40.3 25.2 %copy-start.5 = (bf16[64,2048]{1,0:T(8,128)(2,1)S(1)}, bf16[64,2048]{1,0:T(8,128)(2,1)}, u32[]{:S(2)}) copy-start(bf16[64,2048]{1,0:T(8,128)(2,1)} %weight_ref.1) | copy-start | bytes 786436
  40.3 47.1 %copy-start.2 = (bf16[88,4096]{1,0:T(8,128)(2,1)S(1)}, bf16[88,4096]{1,0:T(8,128)(2,1)}, u32[]{:S(2)}) copy-start(bf16[88,4096]{1,0:T(8,128)(2,1)} %gate_ref.1) | copy-start | bytes 2162692
  40.3 47.1 %copy-start.3 = (bf16[88,4096]{1,0:T(8,128)(2,1)S(1)}, bf16[88,4096]{1,0:T(8,128)(2,1)}, u32[]{:S(2)}) copy-start(bf16[88,4096]{1,0:T(8,128)(2,1)} %up_ref.1) | copy-start | bytes 2162692
  66.1 21.3 %copy-start.6 = (f32[4096]{0:T(1024)S(1)}, f32[4096]{0:T(1024)}, u32[]{:S(2)}) copy-start(f32[4096]{0:T(1024)} %param.21) | copy-start | bytes 49156

commit v6 on v5

--- a/solution.py
+++ b/solution.py
@@ -56,11 +56,8 @@
         copy.wait()
 
 
-def query_kernel(tp_ref, own_ref, other_ref, gain_ref, weight_ref, out_ref):
-    own = own_ref[...].astype(F32)
-    other = other_ref[...].astype(F32)
-    both = jnp.concatenate([own, other, own, other], axis=1)
-    x = jnp.where(tp_ref[0] == 0, both[:, :64], both[:, 32:96])
+def query_kernel(both_ref, gain_ref, weight_ref, out_ref):
+    x = jnp.concatenate([both_ref[0], both_ref[1]], axis=1).astype(F32)
     square = jnp.sum(x * x, axis=1, keepdims=True)
     scaled = (x * gain_ref[:, :64]).astype(BF16)
     q = jnp.dot(scaled, weight_ref[...], preferred_element_type=F32)
@@ -253,7 +250,6 @@
     tp = lax.axis_index("tp").astype(jnp.int32).reshape(1)
     kv = lax.axis_index(KV)
     at = lax.axis_index(KV_TP).astype(jnp.int32).reshape(1)
-    other = lax.ppermute(tokens, "tp", [(0, 1), (1, 0)])
     turn = turn_tables(key_cache.shape[1] * lax.axis_size(KV))
     keys = key_cache.reshape(4, 256, 128)
     values = value_cache.reshape(4, 256, 128)
@@ -288,7 +284,8 @@
         keys,
         values,
     )
-    part = call(query_kernel, "query", (2, 40, 128), F32, tp, own, other, gain, weight, scalars=1)
+    both = lax.all_gather(own, "tp")
+    part = call(query_kernel, "query", (2, 40, 128), F32, both, gain, weight)
     part, at, pair = lax.optimization_barrier((part, at, pair))
     copies = jnp.broadcast_to(part[None], (4, 2, 40, 128)).reshape(8, 40, 128)
     part = jnp.sum(lax.all_to_all(copies, "kv_0", 0, 0, tiled=True), axis=0)

time: 106 us -> 106 us (level)
  starting transfers between devices: 17.6 us -> 8.95 us
  blocking collectives: 76.3 us -> 84.5 us
    ppermute x1 -> x0, starting transfers between devices: 8.73 us -> none  [shards(): other = lax.ppermute(tokens, 'tp', [(0, 1), (1, 0)])]
    all_gather x0 -> x1, blocking collectives: none -> 8.3 us  [shards(): both = lax.all_gather(own, 'tp')]
  transfers between devices with their start and end apart: 3 -> 2, of which waited for: 1 -> 1; matrix products, arithmetic and copies ran while one was open for 0% -> 0% of each run, Pallas kernels for 1% -> 0%
where the time goes in v6:
time: 106 us; the launch traced here: 105 us
  blocking collectives  84.5 us (80%)
  starting transfers between devices  8.95 us (8%)
  waiting for transfers between devices  6.38 us (6%)
  Pallas kernels  4.39 us (4%)
    all_to_all x3, blocking collectives, shared(): return lax.all_to_all(copies, axis, 0, 0, tiled=True)  46.3 us
    all_to_all x1, blocking collectives, shards(): sums = lax.all_to_all(partial.reshape(128, 1, 128), KV_TP, 0, 0, tiled=True)  16.7 us
    all_to_all x1, blocking collectives, shards(): part = jnp.sum(lax.all_to_all(copies, 'kv_0', 0, 0, tiled=True), axis=0)  13.2 us
    all_gather x1, blocking collectives, shards(): both = lax.all_gather(own, 'tp')  8.3 us
    all_to_all x1, starting transfers between devices, shared(): return lax.all_to_all(copies, axis, 0, 0, tiled=True)  6.95 us
    all_to_all x1, waiting for transfers between devices, shared(): return lax.all_to_all(copies, axis, 0, 0, tiled=True)  6.38 us
    pallas_call x6, Pallas kernels, call(): pl.pallas_call(kernel, out_shape=pltpu.VMEM(shape, dtype) if name != 'tot...  3.28 us
  transfers between devices with their start and end apart: 2, of which 1 were waited for; matrix products, arithmetic and copies ran while one was open for 0% of the time, Pallas kernels for 0%

profile of v6, /device:TPU:1, one launch (start us, length us, event | category | flops | bytes accessed | tf_op | source)
XLA Modules:
  0.0 105.2 jit_solution(12403756936168704544)
XLA Ops:
  0.0 1.1 %prepare.1 = (bf16[4,32]{1,0:T(4,128)(2,1)S(1)}, bf16[64,2048]{1,0:T(8,128)(2,1)S(1)}, f32[1,128]{1,0:T(1,128)S(1)}, f32[32,128]{1,0:T(8,128)S(1)}, f32[8,128]{1...) custom-call(s32[1]{0:T(128)} %bitcast.kv_ref, bf16[4,32]{1,0:T(4,128)(2,1)} %own_in.1, ...), custom_call_target="tpu_custom_call" | custom-call | tf_op jit(solution)/shard_map/prepare/pallas_call | solution.py:257
  1.1 8.3 %all-gather.1.both_ref = bf16[2,4,32]{2,1,0:T(4,128)(2,1)S(1)} all-gather(bf16[1,4,32]{2,1,0:T(4,128)(2,1)S(1)} %bitcast.25), channel_id=2, replica_groups=mesh['dp'=4,'kv_0'=8,'kv_1'=8,'tp'=2] {'tp'}, dimensions={0}, use_global_device_ids=true | all-gather | bytes 768 | tf_op jit(solution)/shard_map/all_gather | solution.py:287
  9.4 0.2 shard_map.127
  9.7 13.2 %all_to_all.30 = f32[8,40,128]{2,1,0:T(8,128)S(1)} all-to-all(f32[8,40,128]{2,1,0:T(8,128)S(1)} %bitcast.26), channel_id=1, replica_groups=mesh['dp'=4,'kv_0'=8,'kv_1'=8,'tp'=2] {'kv_0'}, dimensions={0} | all-to-all | bytes 327680 | tf_op jit(solution)/shard_map/all_to_all | solution.py:291
  22.9 0.0 copy-start.1
  22.9 0.7 broadcast_in_dim.19
  23.5 7.0 %all-to-all-start.1 = ((f32[8,40,128]{2,1,0:T(8,128)}), f32[8,40,128]{2,1,0:T(8,128)S(1)}, u32[]{:S(2)}, u32[]{:S(2)}) async-start(f32[8,40,128]{2,1,0:T(8,128)} %broadcast_in_dim.19), calls=%async_computation.1 | async-start | bytes 327680 | tf_op jit(solution)/shard_map/all_to_all | solution.py:33
  30.5 2.0 %collective-permute-start = (bf16[4,256,128]{2,1,0:T(8,128)(2,1)S(1)}, bf16[4,256,128]{2,1,0:T(8,128)(2,1)S(1)}, u32[]{:S(2)}, u32[]{:S(2)}) collective-permute-start(bf16[4,256,128]{2,1,0:T(8,128)(2,1)S(1)} %get-tuple-element.26), channel_id=1, source_target_pairs={{0,16},{16,0},{32,48},{48,32},{64,80},{80,64},{96,112},{112,96},{1... | collective-permute-start | bytes 786440 | tf_op jit(solution)/shard_map/ppermute | solution.py:293
  32.5 6.4 %all-to-all-done.1 = f32[8,40,128]{2,1,0:T(8,128)S(1)} async-done(((f32[8,40,128]{2,1,0:T(8,128)}), f32[8,40,128]{2,1,0:T(8,128)S(1)}, u32[]{:S(2)}, u32[]{:S(2)}) %all-to-all-start.1) | async-done | bytes 163872 | tf_op jit(solution)/shard_map/all_to_all | solution.py:33
  38.9 0.0 collective-permute-done.cache_ref
  38.9 0.0 copy-done.1
  38.9 0.0 copy-done
  38.9 0.0 copy-start.4
  38.9 0.5 shard_map.128
  39.5 0.0 copy-start.5
  39.5 0.0 copy-start.2
  39.5 0.0 copy-start.3
  39.5 13.3 %all_to_all.31.parts_ref = bf16[8,72,128]{2,1,0:T(8,128)(2,1)S(1)} all-to-all(bf16[8,72,128]{2,1,0:T(8,128)(2,1)S(1)} %broadcast_in_dim.20), channel_id=1, replica_groups=mesh['dp'=4,'kv_0'=8,'kv_1'=8,'tp'=2] {'kv_1'}, dimensions={0} | all-to-all | bytes 294912 | tf_op jit(solution)/shard_map/all_to_all | solution.py:33
  52.9 0.3 shard_map.129
  53.2 11.5 %all_to_all.32.parts_ref = bf16[8,72,128]{2,1,0:T(8,128)(2,1)S(1)} all-to-all(bf16[8,72,128]{2,1,0:T(8,128)(2,1)S(1)} %broadcast_in_dim.21), channel_id=1, replica_groups=mesh['dp'=4,'kv_0'=8,'kv_1'=8,'tp'=2] {'kv_0'}, dimensions={0} | all-to-all | bytes 294912 | tf_op jit(solution)/shard_map/all_to_all | solution.py:33
  64.7 0.0 copy-done.5
  64.7 0.6 shard_map.130
  65.3 0.1 broadcast_in_dim.22
  65.4 0.0 copy-start.6
  65.4 21.4 %all_to_all.33 = bf16[128,2,128]{2,1,0:T(2,128)(2,1)S(1)} all-to-all(bf16[128,2,128]{2,1,0:T(2,128)(2,1)S(1)} %broadcast_in_dim.22), channel_id=1, replica_groups=mesh['dp'=4,'kv_0'=8,'kv_1'=8,'tp'=2] {'kv_0','kv_1','tp'}, dimensions={0} | all-to-all | bytes 131072 | tf_op jit(solution)/shard_map/all_to_all | solution.py:33
  86.8 0.0 copy-done.4
  86.8 0.0 copy-done.2
  86.8 0.0 copy-done.3
  86.8 0.0 copy-done.6
  86.8 1.0 shard_map.131
  87.9 16.7 %all_to_all.34 = f32[128,1,128]{2,1,0:T(1,128)S(1)} all-to-all(f32[128,1,128]{2,1,0:T(1,128)S(1)} %bitcast.22), channel_id=1, replica_groups=mesh['dp'=4,'kv_0'=8,'kv_1'=8,'tp'=2] {'kv_0','kv_1','tp'}, dimensions={0} | all-to-all | bytes 131072 | tf_op jit(solution)/shard_map/all_to_all | solution.py:339
  104.5 0.7 shard_map.132
  (6 shorter events, 0.1 us)
Async XLA Ops:
  22.9 16.1 %copy-start.1 = (bf16[4,256,1,128]{3,1,2,0:T(8,128)(2,1)S(1)}, bf16[4,256,1,128]{3,1,2,0:T(8,128)(2,1)}, u32[]{:S(2)}) copy-start(bf16[4,256,1,128]{3,1,2,0:T(8,128)(2,1)} %param.17) | copy-start | bytes 786436
  23.5 15.4 %copy-start = (bf16[4,256,1,128]{3,1,2,0:T(8,128)(2,1)S(1)}, bf16[4,256,1,128]{3,1,2,0:T(8,128)(2,1)}, u32[]{:S(2)}) copy-start(bf16[4,256,1,128]{3,1,2,0:T(8,128)(2,1)} %param.16) | copy-start | bytes 786436
  23.5 15.3 %all-to-all-start.1 = ((f32[8,40,128]{2,1,0:T(8,128)}), f32[8,40,128]{2,1,0:T(8,128)S(1)}, u32[]{:S(2)}, u32[]{:S(2)}) async-start(f32[8,40,128]{2,1,0:T(8,128)} %broadcast_in_dim.19), calls=%async_computation.1 | async-start | bytes 327680 | tf_op jit(solution)/shard_map/all_to_all | solution.py:33
  30.5 8.4 %collective-permute-start = (bf16[4,256,128]{2,1,0:T(8,128)(2,1)S(1)}, bf16[4,256,128]{2,1,0:T(8,128)(2,1)S(1)}, u32[]{:S(2)}, u32[]{:S(2)}) collective-permute-start(bf16[4,256,128]{2,1,0:T(8,128)(2,1)S(1)} %get-tuple-element.26), channel_id=1, source_target_pairs={{0,16},{16,0},{32,48},{48,32},{64,80},{80,64},{96,112},{112,96},{1... | collective-permute-start | bytes 786440 | tf_op jit(solution)/shard_map/ppermute | solution.py:293
  38.9 47.9 %copy-start.4 = (bf16[88,4096]{1,0:T(8,128)(2,1)S(1)}, bf16[88,4096]{1,0:T(8,128)(2,1)}, u32[]{:S(2)}) copy-start(bf16[88,4096]{1,0:T(8,128)(2,1)} %down_ref.1) | copy-start | bytes 2162692
  39.5 25.3 %copy-start.5 = (bf16[64,2048]{1,0:T(8,128)(2,1)S(1)}, bf16[64,2048]{1,0:T(8,128)(2,1)}, u32[]{:S(2)}) copy-start(bf16[64,2048]{1,0:T(8,128)(2,1)} %weight_ref.1) | copy-start | bytes 786436
  39.5 47.3 %copy-start.2 = (bf16[88,4096]{1,0:T(8,128)(2,1)S(1)}, bf16[88,4096]{1,0:T(8,128)(2,1)}, u32[]{:S(2)}) copy-start(bf16[88,4096]{1,0:T(8,128)(2,1)} %gate_ref.1) | copy-start | bytes 2162692
  39.5 47.3 %copy-start.3 = (bf16[88,4096]{1,0:T(8,128)(2,1)S(1)}, bf16[88,4096]{1,0:T(8,128)(2,1)}, u32[]{:S(2)}) copy-start(bf16[88,4096]{1,0:T(8,128)(2,1)} %up_ref.1) | copy-start | bytes 2162692
  65.4 21.4 %copy-start.6 = (f32[4096]{0:T(1024)S(1)}, f32[4096]{0:T(1024)}, u32[]{:S(2)}) copy-start(f32[4096]{0:T(1024)} %param.21) | copy-start | bytes 49156

commit v7 on v6

--- a/solution.py
+++ b/solution.py
@@ -34,26 +34,30 @@
 
 
 def prepare_kernel(
-    kv_ref, own_in, weight_in, gain_in, lam_in, turn_in, head_in, key_in, value_in,
-    own_ref, weight_ref, gain_ref, lam_ref, turn_ref, head_ref, cache_ref, all_ref, row_ref, sems,
+    kv_ref, own_in, weight_in, gain_in, lam_in, turn_in, head_in,
+    own_ref, weight_ref, gain_ref, lam_ref, turn_ref, head_ref, all_ref, row_ref, sems,
 ):
-    away = pl.ds(2 - 2 * (kv_ref[0] // 8 % 2), 2)
     pairs = [
-        (weight_in, weight_ref), (key_in.at[away], cache_ref.at[0:2]),
-        (value_in.at[away], cache_ref.at[2:4]), (own_in, own_ref), (gain_in, all_ref),
-        (lam_in, row_ref), (turn_in, turn_ref), (head_in, head_ref),
+        (weight_in, weight_ref), (own_in, own_ref), (gain_in, all_ref), (lam_in, row_ref),
+        (turn_in, turn_ref), (head_in, head_ref),
     ]
     copies = [pltpu.make_async_copy(a, b, sems.at[k]) for k, (a, b) in enumerate(pairs)]
     for copy in copies:
         copy.start()
-    for copy in copies[3:]:
+    for copy in copies[1:]:
         copy.wait()
     line = all_ref[pl.ds(kv_ref[0] // 2, 1), :]
     gain_ref[...] = jnp.where(kv_ref[0] % 2 == 0, line, pltpu.roll(line, 64, 1))
     picked = jnp.where(lanes((32, 16)) == rows((32, 16)) // 2, row_ref[...], 0.0)
     lam_ref[...] = jnp.broadcast_to(jnp.sum(picked, axis=1, keepdims=True), (32, 128))
-    for copy in copies[:3]:
-        copy.wait()
+    copies[0].wait()
+
+
+def swap_kernel(pair_ref, key_ref, value_ref, out_ref):
+    away = 2 - 2 * pair_ref[0]
+    for b in range(2):
+        out_ref[b] = key_ref[away + b]
+        out_ref[2 + b] = value_ref[away + b]
 
 
 def query_kernel(both_ref, gain_ref, weight_ref, out_ref):
@@ -254,7 +258,7 @@
     keys = key_cache.reshape(4, 256, 128)
     values = value_cache.reshape(4, 256, 128)
     pair = (kv // 8 % 2).astype(jnp.int32).reshape(1)
-    own, weight, gain, lam, turn, head, cache = pl.pallas_call(
+    own, weight, gain, lam, turn, head = pl.pallas_call(
         prepare_kernel,
         name="prepare",
         out_shape=[
@@ -264,14 +268,13 @@
             pltpu.VMEM((32, 128), F32),
             pltpu.VMEM((8, 128), F32),
             pltpu.VMEM((1, 128), F32),
-            pltpu.VMEM((4, 256, 128), BF16),
         ],
-        in_specs=[pl.BlockSpec(memory_space=pltpu.SMEM)] + [pl.BlockSpec(memory_space=pl.ANY)] * 8,
-        out_specs=[pl.BlockSpec(memory_space=pltpu.VMEM)] * 7,
+        in_specs=[pl.BlockSpec(memory_space=pltpu.SMEM)] + [pl.BlockSpec(memory_space=pl.ANY)] * 6,
+        out_specs=[pl.BlockSpec(memory_space=pltpu.VMEM)] * 6,
         scratch_shapes=[
             pltpu.VMEM((32, 128), F32),
             pltpu.VMEM((1, 16), F32),
-            pltpu.SemaphoreType.DMA((8,)),
+            pltpu.SemaphoreType.DMA((6,)),
         ],
     )(
         kv.astype(jnp.int32).reshape(1),
@@ -281,14 +284,14 @@
         head_lambda.reshape(1, 16),
         turn,
         head_gain.reshape(1, 128),
-        keys,
-        values,
     )
     both = lax.all_gather(own, "tp")
     part = call(query_kernel, "query", (2, 40, 128), F32, both, gain, weight)
     part, at, pair = lax.optimization_barrier((part, at, pair))
     copies = jnp.broadcast_to(part[None], (4, 2, 40, 128)).reshape(8, 40, 128)
     part = jnp.sum(lax.all_to_all(copies, "kv_0", 0, 0, tiled=True), axis=0)
+    part, pair = lax.optimization_barrier((part, pair))
+    cache = call(swap_kernel, "swap", (4, 256, 128), BF16, pair, keys, values, scalars=1)
     part, cache = lax.optimization_barrier((part, cache))
     cache = lax.ppermute(cache, "kv_0", [(z, z ^ 1) for z in range(8)])
     parts = shared(part, "kv_1")

time: 106 us -> 106 us (level)
    pallas_call x6 -> x7, Pallas kernels: 3.28 us -> 3.29 us  [call(): pl.pallas_call(kernel, out_shape=pltpu.VMEM(shape, dtype) if name != 'tot...]
where the time goes in v7:
time: 106 us; the launch traced here: 105 us
  blocking collectives  84.6 us (80%)
  starting transfers between devices  8.82 us (8%)
  waiting for transfers between devices  6.38 us (6%)
  Pallas kernels  4.29 us (4%)
    all_to_all x3, blocking collectives, shared(): return lax.all_to_all(copies, axis, 0, 0, tiled=True)  46.3 us
    all_to_all x1, blocking collectives, shards(): sums = lax.all_to_all(partial.reshape(128, 1, 128), KV_TP, 0, 0, tiled=True)  16.7 us
    all_to_all x1, blocking collectives, shards(): part = jnp.sum(lax.all_to_all(copies, 'kv_0', 0, 0, tiled=True), axis=0)  13.3 us
    all_gather x1, blocking collectives, shards(): both = lax.all_gather(own, 'tp')  8.3 us
    all_to_all x1, starting transfers between devices, shared(): return lax.all_to_all(copies, axis, 0, 0, tiled=True)  6.82 us
    all_to_all x1, waiting for transfers between devices, shared(): return lax.all_to_all(copies, axis, 0, 0, tiled=True)  6.38 us
    pallas_call x7, Pallas kernels, call(): pl.pallas_call(kernel, out_shape=pltpu.VMEM(shape, dtype) if name != 'tot...  3.29 us
  transfers between devices with their start and end apart: 2, of which 1 were waited for; matrix products, arithmetic and copies ran while one was open for 0% of the time, Pallas kernels for 0%

profile of v7, /device:TPU:1, one launch (start us, length us, event | category | flops | bytes accessed | tf_op | source)
XLA Modules:
  0.0 105.1 jit_solution(2536698488291906522)
XLA Ops:
  0.0 1.0 prepare.1
  1.0 8.3 %all-gather.1.both_ref = bf16[2,4,32]{2,1,0:T(4,128)(2,1)S(1)} all-gather(bf16[1,4,32]{2,1,0:T(4,128)(2,1)S(1)} %bitcast.25), channel_id=2, replica_groups=mesh['dp'=4,'kv_0'=8,'kv_1'=8,'tp'=2] {'tp'}, dimensions={0}, use_global_device_ids=true | all-gather | bytes 768 | tf_op jit(solution)/shard_map/all_gather | solution.py:288
  9.3 0.2 shard_map.127
  9.5 0.0 copy-start.1
  9.6 0.0 copy-start
  9.6 13.3 %all_to_all.30 = f32[8,40,128]{2,1,0:T(8,128)S(1)} all-to-all(f32[8,40,128]{2,1,0:T(8,128)S(1)} %bitcast.26), channel_id=1, replica_groups=mesh['dp'=4,'kv_0'=8,'kv_1'=8,'tp'=2] {'kv_0'}, dimensions={0} | all-to-all | bytes 327680 | tf_op jit(solution)/shard_map/all_to_all | solution.py:292
  22.9 0.0 copy-done.1
  22.9 0.0 copy-done
  22.9 0.7 broadcast_in_dim.19
  23.6 6.8 %all-to-all-start.1 = ((f32[8,40,128]{2,1,0:T(8,128)}), f32[8,40,128]{2,1,0:T(8,128)S(1)}, u32[]{:S(2)}, u32[]{:S(2)}) async-start(f32[8,40,128]{2,1,0:T(8,128)} %broadcast_in_dim.19), calls=%async_computation.1 | async-start | bytes 327680 | tf_op jit(solution)/shard_map/all_to_all | solution.py:33
  30.4 2.0 %collective-permute-start = (bf16[4,256,128]{2,1,0:T(8,128)(2,1)S(1)}, bf16[4,256,128]{2,1,0:T(8,128)(2,1)S(1)}, u32[]{:S(2)}, u32[]{:S(2)}) collective-permute-start(bf16[4,256,128]{2,1,0:T(8,128)(2,1)S(1)} %shard_map.128), channel_id=1, source_target_pairs={{0,16},{16,0},{32,48},{48,32},{64,80},{80,64},{96,112},{112,96},{1... | collective-permute-start | bytes 786440 | tf_op jit(solution)/shard_map/ppermute | solution.py:296
  32.4 6.4 %all-to-all-done.1 = f32[8,40,128]{2,1,0:T(8,128)S(1)} async-done(((f32[8,40,128]{2,1,0:T(8,128)}), f32[8,40,128]{2,1,0:T(8,128)S(1)}, u32[]{:S(2)}, u32[]{:S(2)}) %all-to-all-start.1) | async-done | bytes 163872 | tf_op jit(solution)/shard_map/all_to_all | solution.py:33
  38.8 0.0 collective-permute-done.cache_ref
  38.8 0.0 copy-start.4
  38.9 0.5 shard_map.129
  39.4 0.0 copy-start.5
  39.4 0.0 copy-start.2
  39.4 0.0 copy-start.3
  39.4 13.4 %all_to_all.31.parts_ref = bf16[8,72,128]{2,1,0:T(8,128)(2,1)S(1)} all-to-all(bf16[8,72,128]{2,1,0:T(8,128)(2,1)S(1)} %broadcast_in_dim.20), channel_id=1, replica_groups=mesh['dp'=4,'kv_0'=8,'kv_1'=8,'tp'=2] {'kv_1'}, dimensions={0} | all-to-all | bytes 294912 | tf_op jit(solution)/shard_map/all_to_all | solution.py:33
  52.8 0.3 shard_map.130
  53.1 11.5 %all_to_all.32.parts_ref = bf16[8,72,128]{2,1,0:T(8,128)(2,1)S(1)} all-to-all(bf16[8,72,128]{2,1,0:T(8,128)(2,1)S(1)} %broadcast_in_dim.21), channel_id=1, replica_groups=mesh['dp'=4,'kv_0'=8,'kv_1'=8,'tp'=2] {'kv_0'}, dimensions={0} | all-to-all | bytes 294912 | tf_op jit(solution)/shard_map/all_to_all | solution.py:33
  64.6 0.0 copy-done.5
  64.6 0.6 shard_map.131
  65.2 0.1 broadcast_in_dim.22
  65.3 0.0 copy-start.6
  65.3 21.4 %all_to_all.33 = bf16[128,2,128]{2,1,0:T(2,128)(2,1)S(1)} all-to-all(bf16[128,2,128]{2,1,0:T(2,128)(2,1)S(1)} %broadcast_in_dim.22), channel_id=1, replica_groups=mesh['dp'=4,'kv_0'=8,'kv_1'=8,'tp'=2] {'kv_0','kv_1','tp'}, dimensions={0} | all-to-all | bytes 131072 | tf_op jit(solution)/shard_map/all_to_all | solution.py:33
  86.7 0.0 copy-done.4
  86.7 0.0 copy-done.2
  86.7 0.0 copy-done.6
  86.7 1.0 shard_map.132
  87.8 16.7 %all_to_all.34 = f32[128,1,128]{2,1,0:T(1,128)S(1)} all-to-all(f32[128,1,128]{2,1,0:T(1,128)S(1)} %bitcast.22), channel_id=1, replica_groups=mesh['dp'=4,'kv_0'=8,'kv_1'=8,'tp'=2] {'kv_0','kv_1','tp'}, dimensions={0} | all-to-all | bytes 131072 | tf_op jit(solution)/shard_map/all_to_all | solution.py:342
  104.5 0.7 shard_map.133
  (7 shorter events, 0.1 us)
Async XLA Ops:
  9.5 13.4 %copy-start.1 = (bf16[4,256,1,128]{3,1,2,0:T(8,128)(2,1)S(1)}, bf16[4,256,1,128]{3,1,2,0:T(8,128)(2,1)}, u32[]{:S(2)}) copy-start(bf16[4,256,1,128]{3,1,2,0:T(8,128)(2,1)} %param.17) | copy-start | bytes 786436
  9.6 13.3 %copy-start = (bf16[4,256,1,128]{3,1,2,0:T(8,128)(2,1)S(1)}, bf16[4,256,1,128]{3,1,2,0:T(8,128)(2,1)}, u32[]{:S(2)}) copy-start(bf16[4,256,1,128]{3,1,2,0:T(8,128)(2,1)} %param.16) | copy-start | bytes 786436
  23.6 15.2 %all-to-all-start.1 = ((f32[8,40,128]{2,1,0:T(8,128)}), f32[8,40,128]{2,1,0:T(8,128)S(1)}, u32[]{:S(2)}, u32[]{:S(2)}) async-start(f32[8,40,128]{2,1,0:T(8,128)} %broadcast_in_dim.19), calls=%async_computation.1 | async-start | bytes 327680 | tf_op jit(solution)/shard_map/all_to_all | solution.py:33
  30.4 8.4 %collective-permute-start = (bf16[4,256,128]{2,1,0:T(8,128)(2,1)S(1)}, bf16[4,256,128]{2,1,0:T(8,128)(2,1)S(1)}, u32[]{:S(2)}, u32[]{:S(2)}) collective-permute-start(bf16[4,256,128]{2,1,0:T(8,128)(2,1)S(1)} %shard_map.128), channel_id=1, source_target_pairs={{0,16},{16,0},{32,48},{48,32},{64,80},{80,64},{96,112},{112,96},{1... | collective-permute-start | bytes 786440 | tf_op jit(solution)/shard_map/ppermute | solution.py:296
  38.8 47.9 %copy-start.4 = (bf16[88,4096]{1,0:T(8,128)(2,1)S(1)}, bf16[88,4096]{1,0:T(8,128)(2,1)}, u32[]{:S(2)}) copy-start(bf16[88,4096]{1,0:T(8,128)(2,1)} %down_ref.1) | copy-start | bytes 2162692
  39.4 25.3 %copy-start.5 = (bf16[64,2048]{1,0:T(8,128)(2,1)S(1)}, bf16[64,2048]{1,0:T(8,128)(2,1)}, u32[]{:S(2)}) copy-start(bf16[64,2048]{1,0:T(8,128)(2,1)} %weight_ref.1) | copy-start | bytes 786436
  39.4 47.3 %copy-start.2 = (bf16[88,4096]{1,0:T(8,128)(2,1)S(1)}, bf16[88,4096]{1,0:T(8,128)(2,1)}, u32[]{:S(2)}) copy-start(bf16[88,4096]{1,0:T(8,128)(2,1)} %gate_ref.1) | copy-start | bytes 2162692
  39.4 47.3 %copy-start.3 = (bf16[88,4096]{1,0:T(8,128)(2,1)S(1)}, bf16[88,4096]{1,0:T(8,128)(2,1)}, u32[]{:S(2)}) copy-start(bf16[88,4096]{1,0:T(8,128)(2,1)} %up_ref.1) | copy-start | bytes 2162692
  65.3 21.4 %copy-start.6 = (f32[4096]{0:T(1024)S(1)}, f32[4096]{0:T(1024)}, u32[]{:S(2)}) copy-start(f32[4096]{0:T(1024)} %param.21) | copy-start | bytes 49156
